TPU v7x, 256 devices: a 4x2x16 block of a 4x16x16 slice. The times are simulated.
256 devices in a mesh: grp: 2 (over y), sp: 16 (over z), fs: 4 (over x), tp: 2 (over core).
Axes of the slice: x: 4, y: 2, z: 16, core: 2. Of those that a mesh axis runs over, the one named last changes fastest.
The devices are a block of a 4x16x16 slice.
Arguments:
- tokens: bfloat16 [4, 24576, 2048], P('fs', ('grp', 'sp'), 'tp'), parts along dimension 1, may hold values from -12 to 12
- norm_gain: float32 [2048], replicated, may hold values from 0.1 to 1.9
- query_weight: bfloat16 [2048, 16, 64], P(None, 'tp'), may hold values from -3 to 3
- key_weight: bfloat16 [2048, 4, 64], P(None, 'tp'), may hold values from -3 to 3
- value_weight: bfloat16 [2048, 4, 64], P(None, 'tp'), may hold values from -0.125 to 0.125
- sink_logit: float32 [16], P('tp'), may hold values from 1 to 6
- pool_weight: bfloat16 [2048, 4, 256], P(None, None, 'tp'), may hold values from -0.125 to 0.125
- attn_out_weight: bfloat16 [16, 64, 2048], P('tp'), may hold values from -0.5 to 0.5
- pool_out_weight: bfloat16 [4, 256, 2048], P(None, 'tp'), may hold values from -0.1875 to 0.1875
Outputs:
- mixed: bfloat16 [4, 24576, 2048], P('fs', ('grp', 'sp', 'tp')), parts along dimension 1
There are 2 independent parts, one for each index of `grp`. A program takes and returns all parts, laid end to end along the dimension named above; an argument that names none is the same for every part. Nothing has to cross between parts.
All inputs are finite; a program needn't handle non-finite values.
Results may differ from a plain program's by a relative error of at most 0.0095.
The roundings to bfloat16 on the way count: a program that leaves them out, or rounds other values in their place, can miss the bound.
Values may be sent and summed in bfloat16 or wider, within the bound.
A program may use at most 128 MiB of HBM per device.

v0:
```python
import jax
import jax.numpy as jnp
from jax import lax
from jax.sharding import PartitionSpec as P

WINDOW = 128


def copy_for_each(shard, axis):
    count = lax.axis_size(axis)
    return lax.all_to_all(
        jnp.broadcast_to(shard[None], (count, *shard.shape)), axis, 0, 0, tiled=True
    )


def in_order(tiles, dim):
    shape = list(tiles.shape[1:])
    shape[dim] *= tiles.shape[0]
    return jnp.moveaxis(tiles, 0, dim).reshape(shape)


def gathered_copies(shard, axis, dim):
    tiles = copy_for_each(shard, axis)
    return in_order(tiles, dim)


def from_behind(value, axis, steps):
    count = lax.axis_size(axis)
    first, last = (max(0, -steps), min(count, count - steps))
    return lax.ppermute(value, axis, [(source, source + steps) for source in range(first, last)])


def split_up(shard, dim, count):
    shape = shard.shape
    tiles = shard.reshape(*shape[:dim], count, shape[dim] // count, *shape[dim + 1 :])
    return jnp.moveaxis(tiles, dim, 0)


def sent_and_summed(shard, axis, dim):
    count = lax.axis_size(axis)
    tiles = lax.all_to_all(split_up(shard, dim, count), axis, 0, 0, tiled=True)
    return jnp.sum(tiles.astype(jnp.float32), axis=0)


def rms_norm(rows, gain):
    values = rows.astype(jnp.float32)
    scale = lax.rsqrt(jnp.mean(values * values, axis=-1, keepdims=True) + 1e-06)
    return (values * scale * gain).astype(jnp.bfloat16)


def attend(query, key, value, key_tail, value_tail, sinks, offset):
    rows = query.shape[0]
    local_kv = key_tail.shape[1]
    head_dim = key_tail.shape[2]
    group = query.shape[1] // (local_kv * head_dim)
    blocks = rows // WINDOW
    qb = query.reshape(blocks, WINDOW, local_kv, group, head_dim)

    def banded(tensor, tail):
        tb = tensor.reshape(blocks, WINDOW, local_kv, head_dim)
        whole = jnp.concatenate([tail, tensor.reshape(rows, local_kv, head_dim)], axis=0)
        before = whole[:rows].reshape(blocks, WINDOW, local_kv, head_dim)
        return jnp.concatenate([before, tb], axis=1)

    kw = banded(key, key_tail)
    vw = banded(value, value_tail)
    qi = jnp.arange(WINDOW, dtype=jnp.int32)[:, None]
    kj = jnp.arange(2 * WINDOW, dtype=jnp.int32)[None, :]
    dist = WINDOW + qi - kj
    inside = (dist >= 0) & (dist < WINDOW)
    key_pos = (
        offset + jnp.arange(blocks, dtype=jnp.int32)[:, None, None] * WINDOW - WINDOW + kj[None]
    )
    mask = inside[None] & (key_pos >= 0)
    scores = jnp.einsum(
        "nqhgd,nkhd->nhgqk", qb, kw, preferred_element_type=jnp.float32
    ) * head_dim ** (-0.5)
    scores = jnp.where(mask[:, None, None], scores, -jnp.inf)
    sink = sinks.reshape(1, local_kv, group, 1, 1)
    top = jnp.maximum(jnp.max(scores, axis=-1, keepdims=True), sink)
    expo = jnp.exp(scores - top)
    total = jnp.sum(expo, axis=-1, keepdims=True) + jnp.exp(sink - top)
    weight = (expo / total).astype(jnp.bfloat16)
    out = jnp.einsum("nhgqk,nkhd->nqhgd", weight, vw, preferred_element_type=jnp.float32)
    return out.reshape(rows, -1).astype(jnp.bfloat16)


def shards(
    tokens,
    norm_gain,
    query_weight,
    key_weight,
    value_weight,
    sink_logit,
    pool_weight,
    attn_out_weight,
    pool_out_weight,
):
    whole = gathered_copies(tokens, "tp", 2)[0]
    rows = whole.shape[0]
    width = whole.shape[1]
    local_kv = key_weight.shape[1]
    head_dim = key_weight.shape[2]
    channels = pool_weight.shape[2]
    normed = rms_norm(whole, norm_gain)
    query = jnp.dot(
        normed, query_weight.reshape(width, -1), preferred_element_type=jnp.float32
    ).astype(jnp.bfloat16)
    key = jnp.dot(normed, key_weight.reshape(width, -1), preferred_element_type=jnp.float32).astype(
        jnp.bfloat16
    )
    value = jnp.dot(
        normed, value_weight.reshape(width, -1), preferred_element_type=jnp.float32
    ).astype(jnp.bfloat16)
    pooled_in = jnp.dot(
        normed, pool_weight.reshape(width, -1), preferred_element_type=jnp.float32
    ).astype(jnp.bfloat16)
    pool_rows = pooled_in.reshape(rows, 4, channels)
    key_rows = key.reshape(rows, local_kv, head_dim)
    value_rows = value.reshape(rows, local_kv, head_dim)
    key_tail, value_tail, pool_tail = from_behind(
        (key_rows[rows - WINDOW :], value_rows[rows - WINDOW :], pool_rows[rows - WINDOW :]),
        "sp",
        1,
    )
    offset = lax.axis_index("sp") * rows
    attended = attend(query, key, value, key_tail, value_tail, sink_logit, offset)
    prefix_total = jnp.sum(pool_rows[:, 3].astype(jnp.float32), axis=0)
    totals = gathered_copies(prefix_total[None], "sp", 0)
    below = jnp.arange(totals.shape[0], dtype=jnp.int32) < lax.axis_index("sp")
    carried = jnp.sum(jnp.where(below[:, None], totals, 0.0), axis=0)
    reaches = jnp.array([2.0, 4.0, 16.0, 1000000000.0], jnp.float32)
    ext = jnp.concatenate([pool_tail, pool_rows], axis=0)
    position = jnp.arange(rows, dtype=jnp.int32)[:, None]
    source = jnp.arange(rows + WINDOW, dtype=jnp.int32)[None, :]
    gap = (position + WINDOW - source).astype(jnp.float32)
    group_ids = jnp.arange(4, dtype=jnp.int32)[:, None, None]
    band = (
        (gap[None] >= 0.0)
        & (gap[None] < reaches[:, None, None])
        & ((group_ids < 3) | (source[None] >= WINDOW))
    )
    sums = jnp.einsum(
        "gij,jgc->igc", band.astype(jnp.bfloat16), ext, preferred_element_type=jnp.float32
    )
    carry_rows = jnp.concatenate([jnp.zeros((3, channels), jnp.float32), carried[None]], axis=0)
    sums = sums + carry_rows[None]
    count = (offset + jnp.arange(1, rows + 1, dtype=jnp.int32)).astype(jnp.float32)
    denom = jnp.minimum(count[:, None], reaches[None, :])[:, :, None]
    pooled = (
        (sums / denom - pool_rows.astype(jnp.float32))
        .astype(jnp.bfloat16)
        .reshape(rows, 4 * channels)
    )
    attn_rows = attn_out_weight.reshape(-1, width)
    pool_weight_rows = pool_out_weight.reshape(-1, width)
    part_sum = jnp.dot(attended, attn_rows, preferred_element_type=jnp.float32)
    result = sent_and_summed(
        (part_sum + jnp.dot(pooled, pool_weight_rows, preferred_element_type=jnp.float32)).astype(
            jnp.bfloat16
        ),
        "tp",
        0,
    )
    return result.astype(jnp.bfloat16)[None]


def solution(mesh):
    in_specs = (
        P("fs", ("grp", "sp"), "tp"),
        P(),
        P(None, "tp", None),
        P(None, "tp", None),
        P(None, "tp", None),
        P("tp"),
        P(None, None, "tp"),
        P("tp", None, None),
        P(None, "tp", None),
    )
    out_specs = P("fs", ("grp", "sp", "tp"), None)
    return jax.shard_map(shards, mesh=mesh, in_specs=in_specs, out_specs=out_specs, check_vma=False)
```

profile of v0, /device:TPU:33, one launch (start us, length us, event | category | flops | bytes accessed | tf_op | source)
XLA Modules:
  0.0 115.6 jit_solution(6304475320778265515)
XLA Ops:
  0.0 2.7 %copy.26 = bf16[768,1024]{0,1:T(8,128)(2,1)} copy(bf16[768,1024]{1,0:T(8,128)(2,1)} %bitcast.105) | data formatting | bytes 3145728 | tf_op jit(solution)/shard_map/broadcast_in_dim | solution.py:12
  2.7 3.3 %broadcast_in_dim.35 = bf16[2,1,768,1024]{2,3,1,0:T(8,128)(2,1)} broadcast(bf16[768,1024]{0,1:T(8,128)(2,1)} %copy.26), dimensions={2,3} | broadcast | bytes 4718592 | tf_op jit(solution)/shard_map/broadcast_in_dim | solution.py:12
  6.0 25.8 %all-to-all-start = ((bf16[2,1,768,1024]{2,3,1,0:T(8,128)(2,1)}), bf16[2,1,768,1024]{2,3,1,0:T(8,128)(2,1)}, u32[]{:S(2)}, u32[]{:S(2)}) async-start(bf16[2,1,768,1024]{2,3,1,0:T(8,128)(2,1)} %broadcast_in_dim.35), calls=%async_computation | async-start | bytes 6291456 | tf_op jit(solution)/shard_map/all_to_all | solution.py:11
  31.8 3.4 %all-to-all-done = bf16[2,1,768,1024]{2,3,1,0:T(8,128)(2,1)} async-done(((bf16[2,1,768,1024]{2,3,1,0:T(8,128)(2,1)}), bf16[2,1,768,1024]{2,3,1,0:T(8,128)(2,1)}, u32[]{:S(2)}, u32[]{:S(2)}) %all-to-all-start) | async-done | bytes 3145760 | tf_op jit(solution)/shard_map/all_to_all | solution.py:11
  35.1 2.6 %fusion.4 = f32[768]{0:T(1024)S(1)} fusion(bf16[2,1,768,1024]{2,3,1,0:T(8,128)(2,1)} %all-to-all-done), kind=kLoop, calls=%fused_computation.6 | loop fusion | flops 4717824 | bytes 3148800 | tf_op jit(solution)/shard_map/reduce_sum | solution.py:47
  37.7 2.7 %fusion.6 = bf16[2,1,768,1024]{2,3,0,1:T(8,128)(2,1)S(1)} fusion(bf16[2,1,768,1024]{2,3,1,0:T(8,128)(2,1)} %all-to-all-done, f32[2,1024]{1,0:T(2,128)S(1)} %mul.56, f32[768]{0:T(1024)S(1)} %add_rsqrt_fusion), kind=kLoop, calls=%fused_computation.8 | loop fusion | flops 6291456 | bytes 6302720 | tf_op jit(solution)/shard_map/convert_element_type | solution.py:48
  40.5 0.0 copy-start.5
  40.5 0.0 copy-start.11
  40.5 0.6 convolution_convert_fusion.2
  41.1 0.6 slice.36
  41.7 2.0 %collective-permute-start = (bf16[128,2,64]{0,2,1:T(8,128)(2,1)}, bf16[128,2,64]{0,2,1:T(8,128)(2,1)}, u32[]{:S(2)}, u32[]{:S(2)}) collective-permute-start(bf16[128,2,64]{0,2,1:T(8,128)(2,1)} %bitcast.5), channel_id=1, source_target_pairs={{0,8},{8,16},{16,24},{24,32},{32,40},{40,48},{48,56},{56,64},{64,7... | collective-permute-start | bytes 98312 | tf_op jit(solution)/shard_map/ppermute | solution.py:30
  43.8 0.6 convolution_convert_fusion.1
  44.4 0.6 slice.37
  45.0 1.9 %collective-permute-start.1 = (bf16[128,2,64]{0,2,1:T(8,128)(2,1)}, bf16[128,2,64]{0,2,1:T(8,128)(2,1)}, u32[]{:S(2)}, u32[]{:S(2)}) collective-permute-start(bf16[128,2,64]{0,2,1:T(8,128)(2,1)} %bitcast.11), channel_id=1, source_target_pairs={{0,8},{8,16},{16,24},{24,32},{32,40},{40,48},{48,56},{56,64},{64,7... | collective-permute-start | bytes 98312 | tf_op jit(solution)/shard_map/ppermute | solution.py:30
  46.9 2.0 %fusion.24 = bf16[768,512]{0,1:T(8,128)(2,1)S(1)} fusion(bf16[768,2048]{0,1:T(8,128)(2,1)S(1)} %bitcast.99, bf16[256,8,4,128]{3,2,1,0:T(4,128)(2,1)S(1)} %bitcast.113), kind=kOutput, calls=%fused_computation.30 | convolution fusion | flops 1611005952 | bytes 6029312 | tf_op jit(solution)/shard_map/dot_general | solution.py:115
  48.8 0.1 convert_reduce_fusion
  48.9 0.8 broadcast_in_dim.39
  49.7 7.6 %all-to-all-start.1 = ((f32[16,1,128]{2,1,0:T(1,128)}), f32[16,1,128]{2,1,0:T(1,128)S(1)}, u32[]{:S(2)}, u32[]{:S(2)}) async-start(f32[16,1,128]{2,1,0:T(1,128)} %broadcast_in_dim.39), calls=%async_computation.1 | async-start | bytes 16384 | tf_op jit(solution)/shard_map/all_to_all | solution.py:11
  57.3 3.8 %collective-permute-start.2 = (bf16[128,4,128]{0,2,1:T(8,128)(2,1)S(1)}, bf16[128,4,128]{0,2,1:T(8,128)(2,1)}, u32[]{:S(2)}, u32[]{:S(2)}) collective-permute-start(bf16[128,4,128]{0,2,1:T(8,128)(2,1)S(1)} %bitcast.110), channel_id=1, source_target_pairs={{0,8},{8,16},{16,24},{24,32},{32,40},{40,48},{48,56},{56,64},{64,7... | collective-permute-start | bytes 393224 | tf_op jit(solution)/shard_map/ppermute | solution.py:30
  61.1 1.5 %broadcast_compare_fusion = pred[768,896]{1,0:T(8,128)(4,1)} fusion(s32[768]{0:T(1024)S(1)} %iota_add_fusion), kind=kLoop, calls=%fused_computation.33 | loop fusion | flops 2064384 | bytes 691200 | tf_op jit(solution)/shard_map/ge | solution.py:139
  62.6 1.8 %subtract_convert_fusion = f32[768,896]{1,0:T(8,128)} fusion(s32[768]{0:T(1024)S(1)} %iota_add_fusion), kind=kLoop, calls=%fused_computation.21 | loop fusion | flops 1376256 | bytes 2755584 | tf_op jit(solution)/shard_map/convert_element_type | solution.py:136
  64.4 0.1 add_compare_fusion
  64.5 0.0 copy-start.9
  64.5 0.0 copy-start.12
  64.5 4.3 %convolution_convert_fusion = bf16[768,512]{1,0:T(8,128)(2,1)} fusion(bf16[768,2048]{0,1:T(8,128)(2,1)S(1)} %bitcast.100, bf16[2048,512]{0,1:T(8,128)(2,1)} %bitcast.114), kind=kOutput, calls=%fused_computation.31 | convolution fusion | flops 1611005952 | bytes 6029312 | tf_op jit(solution)/shard_map/dot_general | solution.py:106
  68.9 0.1 broadcast_or_fusion
  68.9 0.7 broadcast_minimum_fusion
  69.6 0.3 broadcast_and_fusion
  69.9 0.5 iota_compare_fusion.1
  70.4 0.2 reshape.331
  70.6 0.2 reshape.327
  70.9 0.1 max.18
  71.0 3.6 %reshape.342 = bf16[6,128,2,4,64]{4,3,2,1,0:T(4,128)(2,1)} reshape(bf16[768,512]{1,0:T(8,128)(2,1)} %convolution_convert_fusion) | data formatting | bytes 1572864 | tf_op jit(solution)/shard_map/reshape | solution.py:57
  74.7 0.0 all-to-all-done.1
  74.7 0.7 select_reduce_fusion
  75.4 0.8 copy_bitcast_fusion
  76.1 2.7 %fusion.13 = (f32[6,2,4,128]{3,2,1,0:T(4,128)S(1)}, f32[6,2,256,128,4]{3,2,4,1,0:T(8,128)S(1)}) fusion(pred[6,128,256]{1,2,0:T(8,128)(4,1)S(1)} %broadcast_and_fusion, bf16[6,128,2,4,64]{4,3,2,1,0:T(4,128)(2,1)} %reshape.342, bf16[6,128,2,64]{1,3,2,0:T(8,128)(2,1)S(1)} %copy.31, bf16[6,128,2,64]{1,3,2,0:T(8,128)(2,1)S(1)} %copy_bitcast_fusion), kind=kOutput, calls=%fused_computation.19 | convolution fusion | flops 206825472 | bytes 7692288 | tf_op jit(solution)/shard_map/nqhgd,nkhd->nhgqk/dot_general | solution.py:75
  78.8 0.1 broadcast_maximum_fusion
  78.9 1.7 %fusion.8 = f32[6,2,4,128]{3,2,1,0:T(4,128)S(1)} fusion(f32[6,2,256,128,4]{3,2,4,1,0:T(8,128)S(1)} %get-tuple-element.6, f32[6,2,4,128]{3,2,1,0:T(4,128)S(1)} %broadcast_maximum_fusion, pred[6,128,256]{1,2,0:T(8,128)(4,1)S(1)} %broadcast_and_fusion), kind=kLoop, calls=%fused_computation.14 | loop fusion | flops 6285312 | bytes 6537216 | tf_op jit(solution)/shard_map/reduce_sum | solution.py:82
  80.6 0.1 exponential_add_fusion
  80.7 0.8 copy_bitcast_fusion.1
  81.5 1.7 %fusion.30 = bf16[6,128,2,4,64]{1,4,3,2,0:T(8,128)(2,1)S(1)} fusion(f32[6,2,256,128,4]{3,2,4,1,0:T(8,128)S(1)} %get-tuple-element.6, f32[6,2,4,128]{3,2,1,0:T(4,128)S(1)} %exponential_add_fusion, f32[6,2,4,128]{3,2,1,0:T(4,128)S(1)} %broadcast_maximum_fusion, pred[6,128,256]{1,2,0:T(8,128)(4,1)S(1)} %broadcast_and_fusion, ...), kind=kOutput, calls=%fused_computation.34 | convolution fusion | flops 210370560 | bytes 7716864 | tf_op jit(solution)/shard_map/nhgqk,nkhd->nqhgd/dot_general | solution.py:84
  83.2 0.6 copy.35
  83.8 0.0 copy-start.10
  83.8 4.5 %fusion.37 = f32[768,2048]{1,0:T(8,128)} fusion(bf16[512,2048]{1,0:T(8,128)(2,1)S(1)} %bitcast.96, bf16[64,8,6,128]{3,2,1,0:T(8,128)(2,1)S(1)} %bitcast.101), kind=kOutput, calls=%fused_computation.40 | convolution fusion | flops 1610612736 | bytes 9175040 | tf_op jit(solution)/shard_map/dot_general | solution.py:157
  88.3 11.3 %fusion.7 = bf16[768,2048]{1,0:T(8,128)(2,1)} fusion(f32[768,2048]{1,0:T(8,128)} %fusion.37, bf16[4,128,2048]{2,1,0:T(8,128)(2,1)} %param.18, bf16[768,4,128]{0,2,1:T(8,128)(2,1)} %bitcast.109, f32[768,896]{1,0:T(8,128)} %subtract_convert_fusion, f32[4]{0:T(128)S(1)} %copy-done.10, pred[4,896]{1,0:T(4,128)(4,1)S(1)} %broadcast_or_fusion, ...), kind=kOutput, calls=%fused_computation.10 | convolution fusion | flops 2330460160 | bytes 15910416 | tf_op jit(solution)/shard_map/dot_general | solution.py:159
  99.6 11.8 %all_to_all.15 = bf16[2,384,2048]{2,1,0:T(8,128)(2,1)} all-to-all(bf16[2,384,2048]{2,1,0:T(8,128)(2,1)} %bitcast.102), channel_id=1, replica_groups=mesh['grp'=2,'sp'=16,'fs'=4,'tp'=2] {'tp'}, dimensions={0} | all-to-all | bytes 6291456 | tf_op jit(solution)/shard_map/all_to_all | solution.py:41
  111.4 4.2 %reduce_sum.52 = bf16[384,2048]{1,0:T(8,128)(2,1)} reduce(bf16[2,384,2048]{2,1,0:T(8,128)(2,1)} %all_to_all.15, bf16[]{:T(256)} %constant.14.clone.1), dimensions={0}, to_apply=%region_5.6 | reduce | flops 786432 | bytes 4718594 | tf_op jit(solution)/shard_map/reduce_sum | solution.py:42
  (37 shorter events, 0.2 us)
Async XLA Ops:
  0.0 83.8 %copy-start = (bf16[8,64,2048]{2,1,0:T(8,128)(2,1)S(1)}, bf16[8,64,2048]{2,1,0:T(8,128)(2,1)}, u32[]{:S(2)}) copy-start(bf16[8,64,2048]{2,1,0:T(8,128)(2,1)} %param.17) | copy-start | bytes 6291460
  6.0 25.8 %copy-start.8 = (f32[2048]{0:T(1024)S(1)}, f32[2048]{0:T(1024)}, u32[]{:S(2)}) copy-start(f32[2048]{0:T(1024)} %param.11) | copy-start | bytes 24580
  6.0 29.1 %all-to-all-start = ((bf16[2,1,768,1024]{2,3,1,0:T(8,128)(2,1)}), bf16[2,1,768,1024]{2,3,1,0:T(8,128)(2,1)}, u32[]{:S(2)}, u32[]{:S(2)}) async-start(bf16[2,1,768,1024]{2,3,1,0:T(8,128)(2,1)} %broadcast_in_dim.35), calls=%async_computation | async-start | bytes 6291456 | tf_op jit(solution)/shard_map/all_to_all | solution.py:11
  37.7 2.8 %copy-start.4 = (bf16[2048,2,64]{0,2,1:T(8,128)(2,1)S(1)}, bf16[2048,2,64]{0,2,1:T(8,128)(2,1)}, u32[]{:S(2)}) copy-start(bf16[2048,2,64]{0,2,1:T(8,128)(2,1)} %param.14) | copy-start | bytes 1572868
  40.5 6.4 %copy-start.1 = (bf16[2,1,768,1024]{2,3,0,1:T(8,128)(2,1)}, bf16[2,1,768,1024]{2,3,0,1:T(8,128)(2,1)S(1)}, u32[]{:S(2)}) copy-start(bf16[2,1,768,1024]{2,3,0,1:T(8,128)(2,1)S(1)} %fusion.6) | copy-start | bytes 9437188
  40.5 3.3 %copy-start.5 = (bf16[2048,2,64]{0,2,1:T(8,128)(2,1)S(1)}, bf16[2048,2,64]{0,2,1:T(8,128)(2,1)}, u32[]{:S(2)}) copy-start(bf16[2048,2,64]{0,2,1:T(8,128)(2,1)} %param.13) | copy-start | bytes 1572868
  40.5 6.4 %copy-start.11 = (bf16[2048,4,128]{2,1,0:T(4,128)(2,1)S(1)}, bf16[2048,4,128]{2,1,0:T(4,128)(2,1)}, u32[]{:S(2)}) copy-start(bf16[2048,4,128]{2,1,0:T(4,128)(2,1)} %param.16) | copy-start | bytes 6291460
  41.7 38.9 %collective-permute-start = (bf16[128,2,64]{0,2,1:T(8,128)(2,1)}, bf16[128,2,64]{0,2,1:T(8,128)(2,1)}, u32[]{:S(2)}, u32[]{:S(2)}) collective-permute-start(bf16[128,2,64]{0,2,1:T(8,128)(2,1)} %bitcast.5), channel_id=1, source_target_pairs={{0,8},{8,16},{16,24},{24,32},{32,40},{40,48},{48,56},{56,64},{64,7... | collective-permute-start | bytes 98312 | tf_op jit(solution)/shard_map/ppermute | solution.py:30
  45.0 30.4 %collective-permute-start.1 = (bf16[128,2,64]{0,2,1:T(8,128)(2,1)}, bf16[128,2,64]{0,2,1:T(8,128)(2,1)}, u32[]{:S(2)}, u32[]{:S(2)}) collective-permute-start(bf16[128,2,64]{0,2,1:T(8,128)(2,1)} %bitcast.11), channel_id=1, source_target_pairs={{0,8},{8,16},{16,24},{24,32},{32,40},{40,48},{48,56},{56,64},{64,7... | collective-permute-start | bytes 98312 | tf_op jit(solution)/shard_map/ppermute | solution.py:30
  48.8 20.0 %copy-start.6 = (bf16[768,512]{0,1:T(8,128)(2,1)}, bf16[768,512]{0,1:T(8,128)(2,1)S(1)}, u32[]{:S(2)}) copy-start(bf16[768,512]{0,1:T(8,128)(2,1)S(1)} %fusion.24) | copy-start | bytes 2359300
  49.7 24.9 %all-to-all-start.1 = ((f32[16,1,128]{2,1,0:T(1,128)}), f32[16,1,128]{2,1,0:T(1,128)S(1)}, u32[]{:S(2)}, u32[]{:S(2)}) async-start(f32[16,1,128]{2,1,0:T(1,128)} %broadcast_in_dim.39), calls=%async_computation.1 | async-start | bytes 16384 | tf_op jit(solution)/shard_map/all_to_all | solution.py:11
  57.3 31.0 %collective-permute-start.2 = (bf16[128,4,128]{0,2,1:T(8,128)(2,1)S(1)}, bf16[128,4,128]{0,2,1:T(8,128)(2,1)}, u32[]{:S(2)}, u32[]{:S(2)}) collective-permute-start(bf16[128,4,128]{0,2,1:T(8,128)(2,1)S(1)} %bitcast.110), channel_id=1, source_target_pairs={{0,8},{8,16},{16,24},{24,32},{32,40},{40,48},{48,56},{56,64},{64,7... | collective-permute-start | bytes 393224 | tf_op jit(solution)/shard_map/ppermute | solution.py:30
  61.1 3.4 %copy-start.2 = (bf16[2,1,768,1024]{2,3,0,1:T(8,128)(2,1)S(1)}, bf16[2,1,768,1024]{2,3,0,1:T(8,128)(2,1)}, u32[]{:S(2)}) copy-start(bf16[2,1,768,1024]{2,3,0,1:T(8,128)(2,1)} %copy-done.1) | copy-start | bytes 9437188
  64.5 4.4 %copy-start.9 = (f32[4]{0:T(128)S(1)}, f32[4]{0:T(128)}, u32[]{:S(2)}) copy-start(f32[4]{0:T(128)} %constant.40.clone) | copy-start | bytes 52
  64.5 6.4 %copy-start.12 = (f32[8]{0:T(128)S(1)}, f32[8]{0:T(128)}, u32[]{:S(2)}) copy-start(f32[8]{0:T(128)} %param.15) | copy-start | bytes 100
  83.8 4.5 %copy-start.3 = (pred[768,896]{1,0:T(8,128)(4,1)S(1)}, pred[768,896]{1,0:T(8,128)(4,1)}, u32[]{:S(2)}) copy-start(pred[768,896]{1,0:T(8,128)(4,1)} %broadcast_compare_fusion) | copy-start | bytes 2064388
  83.8 4.5 %copy-start.7 = (f32[768,4]{0,1:T(4,128)S(1)}, f32[768,4]{0,1:T(4,128)}, u32[]{:S(2)}) copy-start(f32[768,4]{0,1:T(4,128)} %broadcast_minimum_fusion) | copy-start | bytes 36868
  83.8 4.5 %copy-start.10 = (f32[4]{0:T(128)S(1)}, f32[4]{0:T(128)}, u32[]{:S(2)}) copy-start(f32[4]{0:T(128)} %constant.40.clone) | copy-start | bytes 52
where the time goes:
time: 116 us
  starting transfers between devices  41 us (35%)
  matrix products  27.7 us (24%)
  other arithmetic  18.6 us (16%)
  local copies, waits for them, and re-layouts  12.9 us (11%)
  blocking collectives  11.8 us (10%)
  waiting for transfers between devices  3.38 us (3%)
    all_to_all x2, starting transfers between devices, copy_for_each(): lax.all_to_all(jnp.broadcast_to(shard[None], (count, *shard.shape)), axis...  33.3 us
    all_to_all x1, blocking collectives, sent_and_summed(): tiles = lax.all_to_all(split_up(shard, dim, count), axis, 0, 0, tiled=True)  11.8 us
    dot_general x1, matrix products, shards(): jnp.dot(pooled, pool_weight_rows, preferred_element_type=jnp.float32)  11.3 us
    ppermute x3, starting transfers between devices, from_behind(): lax.ppermute(value, axis, [(source, source + steps) for source in range(f...  7.68 us
    broadcast_in_dim x3, local copies, waits for them, and re-layouts, copy_for_each(): jnp.broadcast_to(shard[None], (count, *shard.shape))  6.79 us
    dot_general x1, matrix products, shards(): part_sum = jnp.dot(attended, attn_rows, preferred_element_type=jnp.float32)  4.48 us
    dot_general x1, matrix products, shards(): jnp.dot(normed, query_weight.reshape(width, -1), preferred_element_type=j...  4.34 us
    reduce_sum x1, other arithmetic, sent_and_summed(): return jnp.sum(tiles.astype(jnp.float32), axis=0)  4.21 us
  transfers between devices with their start and end apart: 5, of which 1 were waited for; matrix products, arithmetic and copies ran while one was open for 27% of the time, Pallas kernels for 0%

commit v1 on v0

v1 whole, which is shorter than its diff:
```python
import functools

import jax
import jax.numpy as jnp
from jax import lax
from jax.experimental import pallas as pl
from jax.experimental.pallas import tpu as pltpu
from jax.sharding import PartitionSpec as P

WINDOW = 128
REACHES = (2, 4, 16)
TAIL = 16
GROUP = 4
CHUNKS = 3
OUT_CHUNKS = 4
NEG = -1e30
BF16 = jnp.bfloat16
F32 = jnp.float32
MESH = pl.DeviceIdType.MESH
NT = (((1,), (1,)), ((), ()))


def kernel(
    tok_hbm, gain_ref, wq_hbm, wk_hbm, wv_hbm, sink_ref, wp_hbm, wa_hbm, wpo_hbm,
    out_hbm,
    tok, nrm, wqkv, wpraw, wp, wo, qt, kx, vt, px, att, l3, bt,
    kin, vin, pin, ktail, vtail, ptail, totout, totin, carryout, carryin,
    own, sendbuf, recvbuf, outbuf,
    tok_sem, w_sem, tsend, trecv, tail_send, tail_recv, tot_send, tot_recv,
    carry_send, carry_recv, out_send, out_recv, out_sem, ready,
):
    me = lax.axis_index("tp")
    other = 1 - me
    z = lax.axis_index("sp")
    nz = lax.axis_size("sp")
    rows, width = nrm.shape
    half = width // 2
    heads = qt.shape[0] // 64
    kv = kx.shape[1] // 64
    group = heads // kv
    nb = rows // WINDOW
    crow = rows // CHUNKS
    gi = lax.rem(z, GROUP)
    base = z - gi

    def tok_copy(c):
        return pltpu.make_async_copy(
            tok_hbm.at[0, pl.ds(c * crow, crow), :],
            tok.at[pl.ds(c * crow, crow), pl.ds(pl.multiple_of(me * half, half), half)],
            tok_sem.at[c],
        )

    qn, kn = wq_hbm.shape[0], wk_hbm.shape[0]
    loads = [
        pltpu.make_async_copy(wp_hbm, wpraw, w_sem.at[0]),
        pltpu.make_async_copy(wq_hbm, wqkv.at[pl.ds(0, qn)], w_sem.at[1]),
        pltpu.make_async_copy(wk_hbm, wqkv.at[pl.ds(qn, kn)], w_sem.at[2]),
        pltpu.make_async_copy(wv_hbm, wqkv.at[pl.ds(qn + kn, kn)], w_sem.at[3]),
        pltpu.make_async_copy(wa_hbm, wo.at[pl.ds(0, qn)], w_sem.at[4]),
        pltpu.make_async_copy(wpo_hbm, wo.at[pl.ds(qn, wo.shape[0] - qn)], w_sem.at[5]),
    ]
    for c in range(CHUNKS):
        tok_copy(c).start()
    for load in loads:
        load.start()

    barrier = pltpu.get_barrier_semaphore()
    pl.semaphore_signal(barrier, inc=1, device_id={"tp": other}, device_id_type=MESH)

    def sends_to(d):
        inside = gi + d < GROUP
        leads = gi == GROUP - 1
        return (inside | leads) & (z + d < nz) if d < GROUP else leads & (z + d < nz)

    def hears_from(d):
        return (d <= gi) | ((d == gi + 1) & (base > 0))

    for d in range(1, GROUP + 1):

        @pl.when(sends_to(d))
        def _():
            pl.semaphore_signal(barrier, inc=1, device_id={"sp": z + d}, device_id_type=MESH)

    behind = gi + jnp.where(base > 0, 1, 0)
    pl.semaphore_wait(barrier, 1 + behind)
    for d in range(1, GROUP + 1):

        @pl.when(hears_from(d))
        def _():
            pl.semaphore_signal(ready.at[d - 1], inc=1, device_id={"sp": z - d}, device_id_type=MESH)

    def tok_send(c):
        return pltpu.make_async_remote_copy(
            src_ref=tok_hbm.at[0, pl.ds(c * crow, crow), :],
            dst_ref=tok.at[pl.ds(c * crow, crow), pl.ds(pl.multiple_of(me * half, half), half)],
            send_sem=tsend.at[c],
            recv_sem=trecv.at[c],
            device_id={"tp": other},
            device_id_type=MESH,
        )

    for c in range(CHUNKS):
        tok_send(c).start()

    loads[0].wait()
    pi = lax.broadcasted_iota(jnp.int32, (256, 256), 0)
    pc = lax.broadcasted_iota(jnp.int32, (256, 256), 1)
    perm = jnp.where(pc == 4 * (pi & 63) + (pi >> 6), 1.0, 0.0).astype(BF16)

    def sort_step(r, _):
        at = pl.multiple_of(r * 512, 512)
        pair = jnp.concatenate(
            [wpraw[pl.ds(at, 256), :], wpraw[pl.ds(at + 256, 256), :]], axis=1
        )
        got = jnp.dot(perm, pair, preferred_element_type=F32).astype(BF16)
        to = pl.multiple_of(r * 128, 128)
        for g in range(4):
            for s in range(2):
                wp[pl.ds(to + 64 * s, 64), pl.ds(128 * g, 128)] = got[
                    64 * g : 64 * g + 64, 128 * s : 128 * s + 128
                ]
        return _

    lax.fori_loop(0, width // 128, sort_step, 0)

    gain = gain_ref[...]
    for load in loads[1:4]:
        load.wait()

    def norm_step(r, _):
        at = pl.multiple_of(r * 16, 16)
        x = tok[pl.ds(at, 16), :].astype(F32)
        scale = lax.rsqrt(jnp.sum(x * x, axis=1, keepdims=True) * (1.0 / width) + 1e-06)
        nrm[pl.ds(at, 16), :] = (x * scale * gain).astype(BF16)
        return _

    for c in range(CHUNKS):
        tok_copy(c).wait()
        tok_send(c).wait_recv()
        lax.fori_loop(c * crow // 16, (c + 1) * crow // 16, norm_step, 0)
        lo = c * crow
        part = nrm[lo : lo + crow, :]
        pooled_in = jnp.dot(part, wp[...], preferred_element_type=F32).astype(BF16)
        px[WINDOW + lo : WINDOW + lo + crow, :] = pooled_in
        for b in range(crow // WINDOW):
            piece = pooled_in[b * WINDOW : (b + 1) * WINDOW, 384:].astype(F32)
            n = c * (crow // WINDOW) + b
            bt[n : n + 1, :] = jnp.sum(piece, axis=0, keepdims=True)
        qkv = lax.dot_general(wqkv[...], part, NT, preferred_element_type=F32)
        qt[:, lo : lo + crow] = (qkv[:qn] * 0.125).astype(BF16)
        kx[WINDOW + lo : WINDOW + lo + crow, :] = jnp.transpose(qkv[qn : qn + kn]).astype(BF16)
        vt[:, WINDOW + lo : WINDOW + lo + crow] = qkv[qn + kn :].astype(BF16)

    total = jnp.sum(bt[0:nb, :], axis=0, keepdims=True)
    totout[...] = jnp.broadcast_to(total, totout.shape)
    ktail[...] = kx[rows : rows + WINDOW, :]
    vtail[...] = vt[:, rows : rows + WINDOW]
    ptail[...] = px[WINDOW + rows - TAIL : WINDOW + rows, 0:384]

    def tail_copy(n):
        src, dst = ((ktail, kin), (vtail, vin), (ptail, pin))[n]
        return pltpu.make_async_remote_copy(
            src_ref=src,
            dst_ref=dst,
            send_sem=tail_send.at[n],
            recv_sem=tail_recv.at[n],
            device_id={"sp": z + 1},
            device_id_type=MESH,
        )

    def tot_copy(d):
        return pltpu.make_async_remote_copy(
            src_ref=totout,
            dst_ref=totin.at[d - 1],
            send_sem=tot_send.at[d - 1],
            recv_sem=tot_recv.at[d - 1],
            device_id={"sp": z + d},
            device_id_type=MESH,
        )

    def carry_copy(d):
        return pltpu.make_async_remote_copy(
            src_ref=carryout,
            dst_ref=carryin,
            send_sem=carry_send.at[d - 1],
            recv_sem=carry_recv,
            device_id={"sp": z + d},
            device_id_type=MESH,
        )

    leads = (gi == GROUP - 1) & (z + 1 < nz)
    for d in range(1, GROUP):

        @pl.when(gi + d < GROUP)
        def _():
            pl.semaphore_wait(ready.at[d - 1], 1)
            tot_copy(d).start()

    @pl.when(leads)
    def _():
        pl.semaphore_wait(ready.at[0], 1)

    @pl.when(z + 1 < nz)
    def _():
        for n in range(3):
            tail_copy(n).start()

    keyi = lax.broadcasted_iota(jnp.int32, (WINDOW, group * WINDOW), 0)
    posi = lax.broadcasted_iota(jnp.int32, (WINDOW, group * WINDOW), 1) & (WINDOW - 1)
    bi = lax.broadcasted_iota(jnp.int32, (WINDOW, 2 * WINDOW), 0)
    bj = lax.broadcasted_iota(jnp.int32, (WINDOW, 2 * WINDOW), 1)
    gap = bi + WINDOW - bj
    bands = [jnp.where((gap >= 0) & (gap < r), 1.0, 0.0).astype(BF16) for r in REACHES]
    bands.append(jnp.where((gap >= 0) & (bj >= WINDOW), 1.0, 0.0).astype(BF16))

    def counts(b):
        first = z * rows + b * WINDOW + 1
        return (lax.broadcasted_iota(jnp.int32, (WINDOW, 1), 0) + first).astype(F32)

    def block(b, first):
        at = b * WINDOW if first else pl.multiple_of(b * WINDOW, WINDOW)
        here = keyi <= posi
        for h in range(kv):
            keys = kx[pl.ds(at, 2 * WINDOW), :]
            qs = jnp.concatenate(
                [
                    qt[64 * (group * h + j) : 64 * (group * h + j + 1), pl.ds(at, WINDOW)]
                    for j in range(group)
                ],
                axis=1,
            )
            blank = jnp.zeros_like(qs)
            qpad = jnp.concatenate([qs if n == h else blank for n in range(kv)], axis=0)
            s = jnp.dot(keys, qpad, preferred_element_type=F32)
            before = s[:WINDOW]
            if first:
                before = before + jnp.where(z > 0, 0.0, NEG)
            s = jnp.where(here, s[WINDOW:], before)
            sink = jnp.concatenate(
                [jnp.full((1, WINDOW), sink_ref[group * h + j], F32) for j in range(group)], axis=1
            )
            top = jnp.maximum(jnp.max(s, axis=0, keepdims=True), sink)
            e = jnp.exp(s - top)
            tot = jnp.sum(e, axis=0, keepdims=True) + jnp.exp(sink - top)
            w = e * (1.0 / tot)
            wt = jnp.concatenate(
                [jnp.where(here, 0.0, w).astype(BF16), jnp.where(here, w, 0.0).astype(BF16)],
                axis=0,
            )
            o = jnp.dot(
                vt[64 * h : 64 * (h + 1), pl.ds(at, 2 * WINDOW)], wt, preferred_element_type=F32
            )
            o = jnp.concatenate(
                [o[:, j * WINDOW : (j + 1) * WINDOW] for j in range(group)], axis=0
            )
            att[pl.ds(at, WINDOW), 64 * group * h : 64 * group * (h + 1)] = jnp.transpose(
                o
            ).astype(BF16)
        count = counts(b)
        for g in range(3):
            near = px[pl.ds(at, 2 * WINDOW), 128 * g : 128 * (g + 1)]
            sums = jnp.dot(bands[g], near, preferred_element_type=F32)
            mean = sums * (1.0 / jnp.minimum(count, float(REACHES[g])))
            att[pl.ds(at, WINDOW), qn + 128 * g : qn + 128 * (g + 1)] = (
                mean - near[WINDOW:].astype(F32)
            ).astype(BF16)
        near = px[pl.ds(at, 2 * WINDOW), 384:512]
        l3[pl.ds(at, WINDOW), :] = jnp.dot(bands[3], near, preferred_element_type=F32)

    px[0:WINDOW, :] = jnp.zeros((WINDOW, px.shape[1]), BF16)
    kx[0:WINDOW, :] = jnp.zeros((WINDOW, kx.shape[1]), BF16)
    vt[:, 0:WINDOW] = jnp.zeros((vt.shape[0], WINDOW), BF16)

    def block_step(i, _):
        block(nb - 1 - i, False)
        return _

    lax.fori_loop(0, nb - 1, block_step, 0)

    @pl.when(z > 0)
    def _():
        for n in range(3):
            tail_copy(n).wait_recv()
        kx[0:WINDOW, :] = kin[...]
        vt[:, 0:WINDOW] = vin[...]
        px[WINDOW - TAIL : WINDOW, 0:384] = pin[...]

    block(0, True)

    for d in range(1, GROUP):

        @pl.when(d <= gi)
        def _():
            tot_copy(d).wait_recv()

        @pl.when(d > gi)
        def _():
            totin[d - 1] = jnp.zeros(totin.shape[1:], F32)

    @pl.when(base > 0)
    def _():
        carry_copy(1).wait_recv()

    @pl.when(base == 0)
    def _():
        carryin[...] = jnp.zeros(carryin.shape, F32)

    carried = carryin[...]
    for d in range(1, GROUP):
        carried = carried + totin[d - 1]

    @pl.when(leads)
    def _():
        carryout[...] = carried + totout[...]
        for d in range(1, GROUP + 1):
            if d > 1:
                pl.semaphore_wait(ready.at[d - 1], 1)
            carry_copy(d).start()

    run = carried[0:1, :]
    for b in range(nb):
        lo = b * WINDOW
        mean = (l3[lo : lo + WINDOW, :] + run) * (1.0 / counts(b))
        run = run + bt[b : b + 1, :]
        att[lo : lo + WINDOW, qn + 384 :] = (
            mean - px[WINDOW + lo : WINDOW + lo + WINDOW, 384:].astype(F32)
        ).astype(BF16)

    orow = rows // 2
    ocol = width // OUT_CHUNKS
    for load in loads[4:]:
        load.wait()

    def out_copy(n):
        cols = pl.ds(n * ocol, ocol)
        return pltpu.make_async_remote_copy(
            src_ref=sendbuf.at[:, cols],
            dst_ref=recvbuf.at[:, cols],
            send_sem=out_send.at[n],
            recv_sem=out_recv.at[n],
            device_id={"tp": other},
            device_id_type=MESH,
        )

    def out_store(n):
        cols = pl.ds(n * ocol, ocol)
        return pltpu.make_async_copy(outbuf.at[:, cols], out_hbm.at[:, cols], out_sem.at[n])

    theirs = pl.ds(pl.multiple_of(other * orow, orow), orow)
    ours = pl.ds(pl.multiple_of(me * orow, orow), orow)
    for n in range(OUT_CHUNKS):
        cols = slice(n * ocol, (n + 1) * ocol)
        sendbuf[:, cols] = jnp.dot(
            att[theirs, :], wo[:, cols], preferred_element_type=F32
        ).astype(BF16)
        out_copy(n).start()
    for n in range(OUT_CHUNKS):
        cols = slice(n * ocol, (n + 1) * ocol)
        own[...] = jnp.dot(att[ours, :], wo[:, cols], preferred_element_type=F32)
        out_copy(n).wait_recv()
        outbuf[:, cols] = (own[...] + recvbuf[:, cols].astype(F32)).astype(BF16)
        out_store(n).start()

    for c in range(CHUNKS):
        tok_send(c).wait_send()
    for d in range(1, GROUP):

        @pl.when(gi + d < GROUP)
        def _():
            tot_copy(d).wait_send()

    @pl.when(z + 1 < nz)
    def _():
        for n in range(3):
            tail_copy(n).wait_send()

    @pl.when(leads)
    def _():
        for d in range(1, GROUP + 1):
            carry_copy(d).wait_send()

    for n in range(OUT_CHUNKS):
        out_copy(n).wait_send()
        out_store(n).wait()


def shards(
    tokens,
    norm_gain,
    query_weight,
    key_weight,
    value_weight,
    sink_logit,
    pool_weight,
    attn_out_weight,
    pool_out_weight,
):
    rows, half = tokens.shape[1:]
    width = 2 * half
    assert lax.axis_size("tp") == 2 and lax.axis_size("sp") % GROUP == 0
    turned = [
        jnp.transpose(w, (1, 2, 0)).reshape(-1, width)
        for w in (query_weight, key_weight, value_weight)
    ]
    qn, kn = turned[0].shape[0], turned[1].shape[0]
    pn = pool_weight.shape[1] * pool_weight.shape[2]
    wp = pool_weight.reshape(-1, pool_weight.shape[2])
    wa = attn_out_weight.reshape(-1, width)
    wpo = pool_out_weight.reshape(-1, width)
    anyspace = pl.BlockSpec(memory_space=pl.ANY)
    vm = pltpu.VMEM
    dma = pltpu.SemaphoreType.DMA
    orow = rows // 2
    out = pl.pallas_call(
        kernel,
        out_shape=jax.ShapeDtypeStruct((orow, width), BF16),
        in_specs=[
            anyspace,
            pl.BlockSpec(memory_space=pltpu.VMEM),
            anyspace,
            anyspace,
            anyspace,
            pl.BlockSpec(memory_space=pltpu.SMEM),
            anyspace,
            anyspace,
            anyspace,
        ],
        out_specs=anyspace,
        scratch_shapes=[
            vm((rows, width), BF16),
            vm((rows, width), BF16),
            vm((qn + 2 * kn, width), BF16),
            vm(wp.shape, BF16),
            vm((width, pn), BF16),
            vm((qn + pn, width), BF16),
            vm((qn, rows), BF16),
            vm((WINDOW + rows, kn), BF16),
            vm((kn, WINDOW + rows), BF16),
            vm((WINDOW + rows, pn), BF16),
            vm((rows, qn + pn), BF16),
            vm((rows, 128), F32),
            vm((8, 128), F32),
            vm((WINDOW, kn), BF16),
            vm((kn, WINDOW), BF16),
            vm((TAIL, 384), BF16),
            vm((WINDOW, kn), BF16),
            vm((kn, WINDOW), BF16),
            vm((TAIL, 384), BF16),
            vm((8, 128), F32),
            vm((GROUP - 1, 8, 128), F32),
            vm((8, 128), F32),
            vm((8, 128), F32),
            vm((orow, width // OUT_CHUNKS), F32),
            vm((orow, width), BF16),
            vm((orow, width), BF16),
            vm((orow, width), BF16),
            dma((CHUNKS,)),
            dma((6,)),
            dma((CHUNKS,)),
            dma((CHUNKS,)),
            dma((3,)),
            dma((3,)),
            dma((GROUP - 1,)),
            dma((GROUP - 1,)),
            dma((GROUP,)),
            dma(()),
            dma((OUT_CHUNKS,)),
            dma((OUT_CHUNKS,)),
            dma((OUT_CHUNKS,)),
            pltpu.SemaphoreType.REGULAR((GROUP,)),
        ],
        compiler_params=pltpu.CompilerParams(
            collective_id=0, has_side_effects=True, vmem_limit_bytes=60 * 1024 * 1024
        ),
    )(tokens, norm_gain.reshape(1, width), *turned, sink_logit, wp, wa, wpo)
    return out[None]


def solution(mesh):
    in_specs = (
        P("fs", ("grp", "sp"), "tp"),
        P(),
        P(None, "tp", None),
        P(None, "tp", None),
        P(None, "tp", None),
        P("tp"),
        P(None, None, "tp"),
        P("tp", None, None),
        P(None, "tp", None),
    )
    out_specs = P("fs", ("grp", "sp", "tp"), None)
    return jax.shard_map(shards, mesh=mesh, in_specs=in_specs, out_specs=out_specs, check_vma=False)
```

time: 116 us -> 52.8 us (0.46)
  Pallas kernels: 0 us -> 49.9 us
  starting transfers between devices: 41 us -> 0 us
  matrix products: 27.7 us -> 0 us
  other arithmetic: 18.6 us -> 0 us
  blocking collectives: 11.8 us -> 0 us
  local copies, waits for them, and re-layouts: 12.9 us -> 2.73 us
  waiting for transfers between devices: 3.38 us -> 0 us
    pallas_call x0 -> x1, Pallas kernels: none -> 49.9 us  [shards(): pl.pallas_call(kernel, out_shape=jax.ShapeDtypeStruct((orow, width), BF16...]
    all_to_all x2 -> x0, starting transfers between devices: 33.3 us -> none  [copy_for_each(): lax.all_to_all(jnp.broadcast_to(shard[None], (count, *shard.shape)), axis...]
    dot_general x8 -> x0, matrix products: 27.7 us -> none  [the longest x1 11.3 us: shards(): jnp.dot(pooled, pool_weight_rows, preferred_element_type=jnp.float32)]
    all_to_all x1 -> x0, blocking collectives: 11.8 us -> none  [sent_and_summed(): tiles = lax.all_to_all(split_up(shard, dim, count), axis, 0, 0, tiled=True)]
    reduce_sum x5 -> x0, other arithmetic: 9.24 us -> none  [the longest x1 4.21 us: sent_and_summed(): return jnp.sum(tiles.astype(jnp.float32), axis=0)]
    ppermute x3 -> x0, starting transfers between devices: 7.68 us -> none  [from_behind(): lax.ppermute(value, axis, [(source, source + steps) for source in range(f...]
    broadcast_in_dim x3 -> x0, local copies, waits for them, and re-layouts: 6.79 us -> none  [copy_for_each(): jnp.broadcast_to(shard[None], (count, *shard.shape))]
    convert_element_type x3 -> x0, other arithmetic: 4.5 us -> none  [the longest x1 2.72 us: rms_norm(): return (values * scale * gain).astype(jnp.bfloat16)]
  transfers between devices with their start and end apart: 5 -> 0, of which waited for: 1 -> 0; matrix products, arithmetic and copies ran while one was open for 27% -> 0% of each run, Pallas kernels for 0% -> 0%
where the time goes in v1:
time: 52.8 us; the launch traced here: 52.6 us
  Pallas kernels  49.9 us (95%)
  local copies, waits for them, and re-layouts  2.73 us (5%)
    pallas_call x1, Pallas kernels, shards(): pl.pallas_call(kernel, out_shape=jax.ShapeDtypeStruct((orow, width), BF16...  49.9 us
    unnamed x1, local copies, waits for them, and re-layouts  2.73 us

profile of v1, /device:TPU:33, one launch (start us, length us, event | category | flops | bytes accessed | tf_op | source)
XLA Modules:
  0.0 52.6 jit_solution(13407400453847364907)
XLA Ops:
  0.0 49.9 %shard_map.91 = bf16[384,2048]{1,0:T(8,128)(2,1)} custom-call(bf16[1,768,1024]{2,1,0:T(8,128)(2,1)} %tok_hbm.1, f32[1,2048]{1,0:T(1,128)} %bitcast.21, bf16[512,2048]{1,0:T(8,128)(2,1)} %bitcast.15, bf16[128,2048]{1,0:T(8,128)(2,1)} %bitcast.19, bf16[128,2048]{1,0:T(8,128)(2,1)} %bitcast.20, f32[8]{0:T(128)} %sink_ref.1, bf16[8192,128]{1,0:T(8,128)(2,1)} %bitcast.16, ...), custom_call_target="tpu_custom_call" | custom-call | tf_op jit(solution)/shard_map/pallas_call | solution.py:414
  49.9 2.7 %copy.11 = bf16[1,384,2048]{2,1,0:T(8,128)(2,1)} copy(bf16[1,384,2048]{2,1,0:T(8,128)(2,1)} %bitcast.14) | data formatting | bytes 3145728

commit v2 on v1

--- a/solution.py
+++ b/solution.py
@@ -12,7 +12,7 @@
 TAIL = 16
 GROUP = 4
 CHUNKS = 3
-OUT_CHUNKS = 4
+OUT_CHUNKS = 2
 NEG = -1e30
 BF16 = jnp.bfloat16
 F32 = jnp.float32
@@ -21,19 +21,21 @@
 
 
 def kernel(
-    tok_hbm, gain_ref, wq_hbm, wk_hbm, wv_hbm, sink_ref, wp_hbm, wa_hbm, wpo_hbm,
-    out_hbm,
-    tok, nrm, wqkv, wpraw, wp, wo, qt, kx, vt, px, att, l3, bt,
+    tok_hbm, gain_hbm, wq_hbm, wk_hbm, wv_hbm, sink_hbm, wp_hbm, wa_hbm, wpo_hbm,
+    outbuf,
+    tok, nrm0, nrm1, nrm2, gain_ref, sink_ref, wqkv, wpraw, wp, wo, qt, kx, vt, px, att, l3, bt,
+    sbuf, pbuf,
     kin, vin, pin, ktail, vtail, ptail, totout, totin, carryout, carryin,
-    own, sendbuf, recvbuf, outbuf,
+    sendbuf, recvbuf,
     tok_sem, w_sem, tsend, trecv, tail_send, tail_recv, tot_send, tot_recv,
-    carry_send, carry_recv, out_send, out_recv, out_sem, ready,
+    carry_send, carry_recv, out_send, out_recv, ready,
 ):
     me = lax.axis_index("tp")
     other = 1 - me
     z = lax.axis_index("sp")
     nz = lax.axis_size("sp")
-    rows, width = nrm.shape
+    rows, width = tok.shape
+    nrm = (nrm0, nrm1, nrm2)
     half = width // 2
     heads = qt.shape[0] // 64
     kv = kx.shape[1] // 64
@@ -58,14 +60,15 @@
         pltpu.make_async_copy(wv_hbm, wqkv.at[pl.ds(qn + kn, kn)], w_sem.at[3]),
         pltpu.make_async_copy(wa_hbm, wo.at[pl.ds(0, qn)], w_sem.at[4]),
         pltpu.make_async_copy(wpo_hbm, wo.at[pl.ds(qn, wo.shape[0] - qn)], w_sem.at[5]),
+        pltpu.make_async_copy(gain_hbm, gain_ref, w_sem.at[6]),
+        pltpu.make_async_copy(sink_hbm, sink_ref, w_sem.at[7]),
     ]
+    barrier = pltpu.get_barrier_semaphore()
+    pl.semaphore_signal(barrier, inc=1, device_id={"tp": other}, device_id_type=MESH)
     for c in range(CHUNKS):
         tok_copy(c).start()
-    for load in loads:
+    for load in (*loads[6:], *loads[:6]):
         load.start()
-
-    barrier = pltpu.get_barrier_semaphore()
-    pl.semaphore_signal(barrier, inc=1, device_id={"tp": other}, device_id_type=MESH)
 
     def sends_to(d):
         inside = gi + d < GROUP
@@ -83,11 +86,6 @@
 
     behind = gi + jnp.where(base > 0, 1, 0)
     pl.semaphore_wait(barrier, 1 + behind)
-    for d in range(1, GROUP + 1):
-
-        @pl.when(hears_from(d))
-        def _():
-            pl.semaphore_signal(ready.at[d - 1], inc=1, device_id={"sp": z - d}, device_id_type=MESH)
 
     def tok_send(c):
         return pltpu.make_async_remote_copy(
@@ -101,13 +99,18 @@
 
     for c in range(CHUNKS):
         tok_send(c).start()
+    for d in range(1, GROUP + 1):
+
+        @pl.when(hears_from(d))
+        def _():
+            pl.semaphore_signal(ready.at[d - 1], inc=1, device_id={"sp": z - d}, device_id_type=MESH)
 
     loads[0].wait()
     pi = lax.broadcasted_iota(jnp.int32, (256, 256), 0)
     pc = lax.broadcasted_iota(jnp.int32, (256, 256), 1)
     perm = jnp.where(pc == 4 * (pi & 63) + (pi >> 6), 1.0, 0.0).astype(BF16)
 
-    def sort_step(r, _):
+    def sort_one(r):
         at = pl.multiple_of(r * 512, 512)
         pair = jnp.concatenate(
             [wpraw[pl.ds(at, 256), :], wpraw[pl.ds(at + 256, 256), :]], axis=1
@@ -119,27 +122,28 @@
                 wp[pl.ds(to + 64 * s, 64), pl.ds(128 * g, 128)] = got[
                     64 * g : 64 * g + 64, 128 * s : 128 * s + 128
                 ]
+
+    def sort_step(r, _):
+        for n in range(4):
+            sort_one(4 * r + n)
         return _
 
-    lax.fori_loop(0, width // 128, sort_step, 0)
-
+    lax.fori_loop(0, width // 512, sort_step, 0)
+
+    for load in (*loads[1:4], *loads[6:]):
+        load.wait()
     gain = gain_ref[...]
-    for load in loads[1:4]:
-        load.wait()
-
-    def norm_step(r, _):
-        at = pl.multiple_of(r * 16, 16)
-        x = tok[pl.ds(at, 16), :].astype(F32)
-        scale = lax.rsqrt(jnp.sum(x * x, axis=1, keepdims=True) * (1.0 / width) + 1e-06)
-        nrm[pl.ds(at, 16), :] = (x * scale * gain).astype(BF16)
-        return _
-
-    for c in range(CHUNKS):
-        tok_copy(c).wait()
-        tok_send(c).wait_recv()
-        lax.fori_loop(c * crow // 16, (c + 1) * crow // 16, norm_step, 0)
+
+    def norm(c):
+        for n in range(crow // 16):
+            x = tok[c * crow + 16 * n : c * crow + 16 * (n + 1), :].astype(F32)
+            mean = jnp.sum(x * x, axis=1, keepdims=True) * (1.0 / width)
+            scale = lax.rsqrt(mean + 1e-06)
+            nrm[c][16 * n : 16 * (n + 1), :] = (x * scale * gain).astype(BF16)
+
+    def project(c):
         lo = c * crow
-        part = nrm[lo : lo + crow, :]
+        part = nrm[c][...]
         pooled_in = jnp.dot(part, wp[...], preferred_element_type=F32).astype(BF16)
         px[WINDOW + lo : WINDOW + lo + crow, :] = pooled_in
         for b in range(crow // WINDOW):
@@ -151,6 +155,17 @@
         kx[WINDOW + lo : WINDOW + lo + crow, :] = jnp.transpose(qkv[qn : qn + kn]).astype(BF16)
         vt[:, WINDOW + lo : WINDOW + lo + crow] = qkv[qn + kn :].astype(BF16)
 
+    tok_copy(0).wait()
+    tok_send(0).wait_recv()
+    norm(0)
+    for c in range(1, CHUNKS):
+        tok_copy(c).wait()
+        tok_send(c).wait_recv()
+    for c in range(CHUNKS):
+        if c + 1 < CHUNKS:
+            norm(c + 1)
+        project(c)
+
     total = jnp.sum(bt[0:nb, :], axis=0, keepdims=True)
     totout[...] = jnp.broadcast_to(total, totout.shape)
     ktail[...] = kx[rows : rows + WINDOW, :]
@@ -217,65 +232,77 @@
         first = z * rows + b * WINDOW + 1
         return (lax.broadcasted_iota(jnp.int32, (WINDOW, 1), 0) + first).astype(F32)
 
-    def block(b, first):
-        at = b * WINDOW if first else pl.multiple_of(b * WINDOW, WINDOW)
-        here = keyi <= posi
-        for h in range(kv):
-            keys = kx[pl.ds(at, 2 * WINDOW), :]
-            qs = jnp.concatenate(
-                [
-                    qt[64 * (group * h + j) : 64 * (group * h + j + 1), pl.ds(at, WINDOW)]
-                    for j in range(group)
-                ],
-                axis=1,
-            )
-            blank = jnp.zeros_like(qs)
-            qpad = jnp.concatenate([qs if n == h else blank for n in range(kv)], axis=0)
-            s = jnp.dot(keys, qpad, preferred_element_type=F32)
-            before = s[:WINDOW]
-            if first:
-                before = before + jnp.where(z > 0, 0.0, NEG)
-            s = jnp.where(here, s[WINDOW:], before)
-            sink = jnp.concatenate(
-                [jnp.full((1, WINDOW), sink_ref[group * h + j], F32) for j in range(group)], axis=1
-            )
+    here = keyi <= posi
+    quarter = here[:, :WINDOW]
+
+    def scores(n, b, h):
+        lo = b * WINDOW
+        qs = jnp.concatenate(
+            [
+                qt[64 * (group * h + j) : 64 * (group * h + j + 1), lo : lo + WINDOW]
+                for j in range(group)
+            ],
+            axis=1,
+        )
+        blank = jnp.zeros_like(qs)
+        qpad = jnp.concatenate([qs if i == h else blank for i in range(kv)], axis=0)
+        s = jnp.dot(kx[lo : lo + 2 * WINDOW, :], qpad, preferred_element_type=F32)
+        before = s[:WINDOW]
+        if b == 0:
+            before = before + jnp.where(z > 0, 0.0, NEG)
+        sbuf[n] = jnp.where(here, s[WINDOW:], before)
+
+    def weights(n, b, h):
+        for j in range(group):
+            s = sbuf[n, :, j * WINDOW : (j + 1) * WINDOW]
+            sink = jnp.full((1, WINDOW), sink_ref[group * h + j], F32)
             top = jnp.maximum(jnp.max(s, axis=0, keepdims=True), sink)
             e = jnp.exp(s - top)
             tot = jnp.sum(e, axis=0, keepdims=True) + jnp.exp(sink - top)
-            w = e * (1.0 / tot)
-            wt = jnp.concatenate(
-                [jnp.where(here, 0.0, w).astype(BF16), jnp.where(here, w, 0.0).astype(BF16)],
-                axis=0,
-            )
-            o = jnp.dot(
-                vt[64 * h : 64 * (h + 1), pl.ds(at, 2 * WINDOW)], wt, preferred_element_type=F32
-            )
-            o = jnp.concatenate(
-                [o[:, j * WINDOW : (j + 1) * WINDOW] for j in range(group)], axis=0
-            )
-            att[pl.ds(at, WINDOW), 64 * group * h : 64 * group * (h + 1)] = jnp.transpose(
-                o
-            ).astype(BF16)
+            pbuf[n, :, j * WINDOW : (j + 1) * WINDOW] = (e * (1.0 / tot)).astype(BF16)
+
+    def attend(n, b, h):
+        lo = b * WINDOW
+        w = pbuf[n]
+        blank = jnp.zeros_like(w)
+        wt = jnp.concatenate([jnp.where(here, blank, w), jnp.where(here, w, blank)], axis=0)
+        o = jnp.dot(
+            vt[64 * h : 64 * (h + 1), lo : lo + 2 * WINDOW], wt, preferred_element_type=F32
+        )
+        o = jnp.concatenate([o[:, j * WINDOW : (j + 1) * WINDOW] for j in range(group)], axis=0)
+        att[lo : lo + WINDOW, 64 * group * h : 64 * group * (h + 1)] = jnp.transpose(o).astype(BF16)
+
+    def pool(b):
+        lo = b * WINDOW
         count = counts(b)
         for g in range(3):
-            near = px[pl.ds(at, 2 * WINDOW), 128 * g : 128 * (g + 1)]
+            near = px[lo : lo + 2 * WINDOW, 128 * g : 128 * (g + 1)]
             sums = jnp.dot(bands[g], near, preferred_element_type=F32)
             mean = sums * (1.0 / jnp.minimum(count, float(REACHES[g])))
-            att[pl.ds(at, WINDOW), qn + 128 * g : qn + 128 * (g + 1)] = (
+            att[lo : lo + WINDOW, qn + 128 * g : qn + 128 * (g + 1)] = (
                 mean - near[WINDOW:].astype(F32)
             ).astype(BF16)
-        near = px[pl.ds(at, 2 * WINDOW), 384:512]
-        l3[pl.ds(at, WINDOW), :] = jnp.dot(bands[3], near, preferred_element_type=F32)
+        near = px[lo : lo + 2 * WINDOW, 384:512]
+        l3[lo : lo + WINDOW, :] = jnp.dot(bands[3], near, preferred_element_type=F32)
+
+    def blocks(which):
+        chains = [(b, h) for b in which for h in range(kv)]
+        last = len(chains)
+        for n in range(last + 2):
+            if n < last:
+                scores(n, *chains[n])
+            if 0 <= n - 1 < last:
+                weights(n - 1, *chains[n - 1])
+            if 0 <= n - 2 < last:
+                attend(n - 2, *chains[n - 2])
+                if chains[n - 2][1] == 0:
+                    pool(chains[n - 2][0])
 
     px[0:WINDOW, :] = jnp.zeros((WINDOW, px.shape[1]), BF16)
     kx[0:WINDOW, :] = jnp.zeros((WINDOW, kx.shape[1]), BF16)
     vt[:, 0:WINDOW] = jnp.zeros((vt.shape[0], WINDOW), BF16)
 
-    def block_step(i, _):
-        block(nb - 1 - i, False)
-        return _
-
-    lax.fori_loop(0, nb - 1, block_step, 0)
+    blocks(range(nb - 1, nb // 2 - 1, -1))
 
     @pl.when(z > 0)
     def _():
@@ -285,7 +312,7 @@
         vt[:, 0:WINDOW] = vin[...]
         px[WINDOW - TAIL : WINDOW, 0:384] = pin[...]
 
-    block(0, True)
+    blocks(range(nb // 2 - 1, -1, -1))
 
     for d in range(1, GROUP):
 
@@ -328,7 +355,7 @@
 
     orow = rows // 2
     ocol = width // OUT_CHUNKS
-    for load in loads[4:]:
+    for load in loads[4:6]:
         load.wait()
 
     def out_copy(n):
@@ -341,10 +368,6 @@
             device_id={"tp": other},
             device_id_type=MESH,
         )
-
-    def out_store(n):
-        cols = pl.ds(n * ocol, ocol)
-        return pltpu.make_async_copy(outbuf.at[:, cols], out_hbm.at[:, cols], out_sem.at[n])
 
     theirs = pl.ds(pl.multiple_of(other * orow, orow), orow)
     ours = pl.ds(pl.multiple_of(me * orow, orow), orow)
@@ -356,10 +379,9 @@
         out_copy(n).start()
     for n in range(OUT_CHUNKS):
         cols = slice(n * ocol, (n + 1) * ocol)
-        own[...] = jnp.dot(att[ours, :], wo[:, cols], preferred_element_type=F32)
         out_copy(n).wait_recv()
-        outbuf[:, cols] = (own[...] + recvbuf[:, cols].astype(F32)).astype(BF16)
-        out_store(n).start()
+        own = jnp.dot(att[ours, :], wo[:, cols], preferred_element_type=F32)
+        outbuf[:, cols] = (own + recvbuf[:, cols].astype(F32)).astype(BF16)
 
     for c in range(CHUNKS):
         tok_send(c).wait_send()
@@ -381,7 +403,6 @@
 
     for n in range(OUT_CHUNKS):
         out_copy(n).wait_send()
-        out_store(n).wait()
 
 
 def shards(
@@ -413,22 +434,16 @@
     orow = rows // 2
     out = pl.pallas_call(
         kernel,
-        out_shape=jax.ShapeDtypeStruct((orow, width), BF16),
-        in_specs=[
-            anyspace,
-            pl.BlockSpec(memory_space=pltpu.VMEM),
-            anyspace,
-            anyspace,
-            anyspace,
-            pl.BlockSpec(memory_space=pltpu.SMEM),
-            anyspace,
-            anyspace,
-            anyspace,
-        ],
-        out_specs=anyspace,
+        out_shape=pltpu.VMEM((orow, width), BF16),
+        in_specs=[anyspace] * 9,
+        out_specs=pl.BlockSpec(memory_space=pltpu.VMEM),
         scratch_shapes=[
             vm((rows, width), BF16),
-            vm((rows, width), BF16),
+            vm((rows // CHUNKS, width), BF16),
+            vm((rows // CHUNKS, width), BF16),
+            vm((rows // CHUNKS, width), BF16),
+            vm((1, width), F32),
+            pltpu.SMEM(sink_logit.shape, F32),
             vm((qn + 2 * kn, width), BF16),
             vm(wp.shape, BF16),
             vm((width, pn), BF16),
@@ -440,6 +455,8 @@
             vm((rows, qn + pn), BF16),
             vm((rows, 128), F32),
             vm((8, 128), F32),
+            vm((6, WINDOW, 512), F32),
+            vm((6, WINDOW, 512), BF16),
             vm((WINDOW, kn), BF16),
             vm((kn, WINDOW), BF16),
             vm((TAIL, 384), BF16),
@@ -450,12 +467,10 @@
             vm((GROUP - 1, 8, 128), F32),
             vm((8, 128), F32),
             vm((8, 128), F32),
-            vm((orow, width // OUT_CHUNKS), F32),
-            vm((orow, width), BF16),
             vm((orow, width), BF16),
             vm((orow, width), BF16),
             dma((CHUNKS,)),
-            dma((6,)),
+            dma((8,)),
             dma((CHUNKS,)),
             dma((CHUNKS,)),
             dma((3,)),
@@ -464,7 +479,6 @@
             dma((GROUP - 1,)),
             dma((GROUP,)),
             dma(()),
-            dma((OUT_CHUNKS,)),
             dma((OUT_CHUNKS,)),
             dma((OUT_CHUNKS,)),
             pltpu.SemaphoreType.REGULAR((GROUP,)),

time: 52.8 us -> 39.4 us (0.75)
  Pallas kernels: 49.9 us -> 38.2 us
  local copies, waits for them, and re-layouts: 2.73 us -> 1.15 us
    pallas_call x1, Pallas kernels: 49.9 us -> 38.2 us  [shards(): pl.pallas_call(kernel, out_shape=pltpu.VMEM((orow, width), BF16), in_spec...]
    unnamed x1, local copies, waits for them, and re-layouts: 2.73 us -> 1.15 us
where the time goes in v2:
time: 39.4 us; the launch traced here: 39.3 us
  Pallas kernels  38.2 us (97%)
  local copies, waits for them, and re-layouts  1.15 us (3%)
    pallas_call x1, Pallas kernels, shards(): pl.pallas_call(kernel, out_shape=pltpu.VMEM((orow, width), BF16), in_spec...  38.2 us
    unnamed x1, local copies, waits for them, and re-layouts  1.15 us

profile of v2, /device:TPU:33, one launch (start us, length us, event | category | flops | bytes accessed | tf_op | source)
XLA Modules:
  0.0 39.3 jit_solution(16400862089510849300)
XLA Ops:
  0.0 38.2 %shard_map.91 = bf16[384,2048]{1,0:T(8,128)(2,1)S(1)} custom-call(bf16[1,768,1024]{2,1,0:T(8,128)(2,1)} %tok_hbm.1, f32[1,2048]{1,0:T(1,128)} %bitcast.21, bf16[512,2048]{1,0:T(8,128)(2,1)} %bitcast.15, bf16[128,2048]{1,0:T(8,128)(2,1)} %bitcast.19, bf16[128,2048]{1,0:T(8,128)(2,1)} %bitcast.20, f32[8]{0:T(128)} %sink_hbm.1, bf16[8192,128]{1,0:T(8,128)(2,1)} %bitcast.16, ...), custom_call_target="tpu_custom_call" | custom-call | tf_op jit(solution)/shard_map/pallas_call | solution.py:435
  38.2 1.1 %copy.11 = bf16[1,384,2048]{2,1,0:T(8,128)(2,1)} copy(bf16[1,384,2048]{2,1,0:T(8,128)(2,1)S(1)} %bitcast.14) | data formatting | bytes 3145728

commit v3 on v2

--- a/solution.py
+++ b/solution.py
@@ -26,7 +26,7 @@
     tok, nrm0, nrm1, nrm2, gain_ref, sink_ref, wqkv, wpraw, wp, wo, qt, kx, vt, px, att, l3, bt,
     sbuf, pbuf,
     kin, vin, pin, ktail, vtail, ptail, totout, totin, carryout, carryin,
-    sendbuf, recvbuf,
+    own0, own1, sendbuf, recvbuf,
     tok_sem, w_sem, tsend, trecv, tail_send, tail_recv, tot_send, tot_recv,
     carry_send, carry_recv, out_send, out_recv, ready,
 ):
@@ -36,6 +36,7 @@
     nz = lax.axis_size("sp")
     rows, width = tok.shape
     nrm = (nrm0, nrm1, nrm2)
+    own = (own0, own1)
     half = width // 2
     heads = qt.shape[0] // 64
     kv = kx.shape[1] // 64
@@ -65,9 +66,9 @@
     ]
     barrier = pltpu.get_barrier_semaphore()
     pl.semaphore_signal(barrier, inc=1, device_id={"tp": other}, device_id_type=MESH)
-    for c in range(CHUNKS):
+    for c in reversed(range(CHUNKS)):
         tok_copy(c).start()
-    for load in (*loads[6:], *loads[:6]):
+    for load in (*loads[6:], *loads[1:4], loads[0], *loads[4:6]):
         load.start()
 
     def sends_to(d):
@@ -97,7 +98,7 @@
             device_id_type=MESH,
         )
 
-    for c in range(CHUNKS):
+    for c in reversed(range(CHUNKS)):
         tok_send(c).start()
     for d in range(1, GROUP + 1):
 
@@ -105,7 +106,6 @@
         def _():
             pl.semaphore_signal(ready.at[d - 1], inc=1, device_id={"sp": z - d}, device_id_type=MESH)
 
-    loads[0].wait()
     pi = lax.broadcasted_iota(jnp.int32, (256, 256), 0)
     pc = lax.broadcasted_iota(jnp.int32, (256, 256), 1)
     perm = jnp.where(pc == 4 * (pi & 63) + (pi >> 6), 1.0, 0.0).astype(BF16)
@@ -123,17 +123,6 @@
                     64 * g : 64 * g + 64, 128 * s : 128 * s + 128
                 ]
 
-    def sort_step(r, _):
-        for n in range(4):
-            sort_one(4 * r + n)
-        return _
-
-    lax.fori_loop(0, width // 512, sort_step, 0)
-
-    for load in (*loads[1:4], *loads[6:]):
-        load.wait()
-    gain = gain_ref[...]
-
     def norm(c):
         for n in range(crow // 16):
             x = tok[c * crow + 16 * n : c * crow + 16 * (n + 1), :].astype(F32)
@@ -141,36 +130,27 @@
             scale = lax.rsqrt(mean + 1e-06)
             nrm[c][16 * n : 16 * (n + 1), :] = (x * scale * gain).astype(BF16)
 
-    def project(c):
+    def pool_in(c):
         lo = c * crow
-        part = nrm[c][...]
-        pooled_in = jnp.dot(part, wp[...], preferred_element_type=F32).astype(BF16)
+        pooled_in = jnp.dot(nrm[c][...], wp[...], preferred_element_type=F32).astype(BF16)
         px[WINDOW + lo : WINDOW + lo + crow, :] = pooled_in
         for b in range(crow // WINDOW):
             piece = pooled_in[b * WINDOW : (b + 1) * WINDOW, 384:].astype(F32)
             n = c * (crow // WINDOW) + b
             bt[n : n + 1, :] = jnp.sum(piece, axis=0, keepdims=True)
-        qkv = lax.dot_general(wqkv[...], part, NT, preferred_element_type=F32)
-        qt[:, lo : lo + crow] = (qkv[:qn] * 0.125).astype(BF16)
-        kx[WINDOW + lo : WINDOW + lo + crow, :] = jnp.transpose(qkv[qn : qn + kn]).astype(BF16)
-        vt[:, WINDOW + lo : WINDOW + lo + crow] = qkv[qn + kn :].astype(BF16)
-
-    tok_copy(0).wait()
-    tok_send(0).wait_recv()
-    norm(0)
-    for c in range(1, CHUNKS):
-        tok_copy(c).wait()
-        tok_send(c).wait_recv()
-    for c in range(CHUNKS):
-        if c + 1 < CHUNKS:
-            norm(c + 1)
-        project(c)
-
-    total = jnp.sum(bt[0:nb, :], axis=0, keepdims=True)
-    totout[...] = jnp.broadcast_to(total, totout.shape)
-    ktail[...] = kx[rows : rows + WINDOW, :]
-    vtail[...] = vt[:, rows : rows + WINDOW]
-    ptail[...] = px[WINDOW + rows - TAIL : WINDOW + rows, 0:384]
+
+    def qkv_of(c):
+        lo = c * crow
+        cut = (qn + 2 * kn) // 2
+        part = nrm[c][...]
+        q = lax.dot_general(wqkv[:cut, :], part, NT, preferred_element_type=F32)
+        qkv = lax.dot_general(wqkv[cut:, :], part, NT, preferred_element_type=F32)
+        qt[:cut, lo : lo + crow] = (q * 0.125).astype(BF16)
+        qt[cut:, lo : lo + crow] = (qkv[: qn - cut] * 0.125).astype(BF16)
+        kx[WINDOW + lo : WINDOW + lo + crow, :] = jnp.transpose(
+            qkv[qn - cut : qn - cut + kn]
+        ).astype(BF16)
+        vt[:, WINDOW + lo : WINDOW + lo + crow] = qkv[qn - cut + kn :].astype(BF16)
 
     def tail_copy(n):
         src, dst = ((ktail, kin), (vtail, vin), (ptail, pin))[n]
@@ -204,21 +184,6 @@
         )
 
     leads = (gi == GROUP - 1) & (z + 1 < nz)
-    for d in range(1, GROUP):
-
-        @pl.when(gi + d < GROUP)
-        def _():
-            pl.semaphore_wait(ready.at[d - 1], 1)
-            tot_copy(d).start()
-
-    @pl.when(leads)
-    def _():
-        pl.semaphore_wait(ready.at[0], 1)
-
-    @pl.when(z + 1 < nz)
-    def _():
-        for n in range(3):
-            tail_copy(n).start()
 
     keyi = lax.broadcasted_iota(jnp.int32, (WINDOW, group * WINDOW), 0)
     posi = lax.broadcasted_iota(jnp.int32, (WINDOW, group * WINDOW), 1) & (WINDOW - 1)
@@ -285,24 +250,71 @@
         near = px[lo : lo + 2 * WINDOW, 384:512]
         l3[lo : lo + WINDOW, :] = jnp.dot(bands[3], near, preferred_element_type=F32)
 
-    def blocks(which):
+    def blocks(which, beside=()):
         chains = [(b, h) for b in which for h in range(kv)]
         last = len(chains)
+        beside = list(beside)
         for n in range(last + 2):
             if n < last:
                 scores(n, *chains[n])
             if 0 <= n - 1 < last:
                 weights(n - 1, *chains[n - 1])
+            if n % 2 == 1 and beside:
+                step, chunk = beside.pop(0)
+                step(chunk)
             if 0 <= n - 2 < last:
                 attend(n - 2, *chains[n - 2])
                 if chains[n - 2][1] == 0:
                     pool(chains[n - 2][0])
 
+    loads[6].wait()
+    gain = gain_ref[...]
+    tok_copy(2).wait()
+    tok_send(2).wait_recv()
+    norm(2)
+    tok_copy(1).wait()
+    tok_send(1).wait_recv()
+    for load in loads[1:4]:
+        load.wait()
+
+    norm(1)
+    qkv_of(2)
+
+    tok_copy(0).wait()
+    tok_send(0).wait_recv()
+    loads[0].wait()
+    norm(0)
+    for r in range(width // 128):
+        sort_one(r)
+    qkv_of(1)
+    pool_in(2)
+
+    ktail[...] = kx[rows : rows + WINDOW, :]
+    vtail[...] = vt[:, rows : rows + WINDOW]
+    ptail[...] = px[WINDOW + rows - TAIL : WINDOW + rows, 0:384]
     px[0:WINDOW, :] = jnp.zeros((WINDOW, px.shape[1]), BF16)
     kx[0:WINDOW, :] = jnp.zeros((WINDOW, kx.shape[1]), BF16)
     vt[:, 0:WINDOW] = jnp.zeros((vt.shape[0], WINDOW), BF16)
 
-    blocks(range(nb - 1, nb // 2 - 1, -1))
+    @pl.when(z + 1 < nz)
+    def _():
+        pl.semaphore_wait(ready.at[0], 1)
+        for n in range(3):
+            tail_copy(n).start()
+
+    loads[7].wait()
+
+    blocks(range(nb - 1, nb // 2 - 1, -1), ((pool_in, 1), (qkv_of, 0), (pool_in, 0)))
+
+    total = jnp.sum(bt[0:nb, :], axis=0, keepdims=True)
+    totout[...] = jnp.broadcast_to(total, totout.shape)
+    for d in range(1, GROUP):
+
+        @pl.when(gi + d < GROUP)
+        def _():
+            if d > 1:
+                pl.semaphore_wait(ready.at[d - 1], 1)
+            tot_copy(d).start()
 
     @pl.when(z > 0)
     def _():
@@ -377,11 +389,16 @@
             att[theirs, :], wo[:, cols], preferred_element_type=F32
         ).astype(BF16)
         out_copy(n).start()
+    def add(n):
+        cols = slice(n * ocol, (n + 1) * ocol)
+        outbuf[:, cols] = (own[n][...] + recvbuf[:, cols].astype(F32)).astype(BF16)
+
     for n in range(OUT_CHUNKS):
         cols = slice(n * ocol, (n + 1) * ocol)
+        own[n][...] = jnp.dot(att[ours, :], wo[:, cols], preferred_element_type=F32)
+    for n in range(OUT_CHUNKS):
         out_copy(n).wait_recv()
-        own = jnp.dot(att[ours, :], wo[:, cols], preferred_element_type=F32)
-        outbuf[:, cols] = (own + recvbuf[:, cols].astype(F32)).astype(BF16)
+        add(n)
 
     for c in range(CHUNKS):
         tok_send(c).wait_send()
@@ -467,6 +484,8 @@
             vm((GROUP - 1, 8, 128), F32),
             vm((8, 128), F32),
             vm((8, 128), F32),
+            vm((orow, width // OUT_CHUNKS), F32),
+            vm((orow, width // OUT_CHUNKS), F32),
             vm((orow, width), BF16),
             vm((orow, width), BF16),
             dma((CHUNKS,)),

time: 39.4 us -> 37.3 us (0.947)
  Pallas kernels: 38.2 us -> 36 us
    pallas_call x1, Pallas kernels: 38.2 us -> 36 us  [shards(): pl.pallas_call(kernel, out_shape=pltpu.VMEM((orow, width), BF16), in_spec...]
where the time goes in v3:
time: 37.3 us; the launch traced here: 37.2 us
  Pallas kernels  36 us (97%)
  local copies, waits for them, and re-layouts  1.15 us (3%)
    pallas_call x1, Pallas kernels, shards(): pl.pallas_call(kernel, out_shape=pltpu.VMEM((orow, width), BF16), in_spec...  36 us
    unnamed x1, local copies, waits for them, and re-layouts  1.15 us

profile of v3, /device:TPU:33, one launch (start us, length us, event | category | flops | bytes accessed | tf_op | source)
XLA Modules:
  0.0 37.2 jit_solution(919400402797315001)
XLA Ops:
  0.0 36.0 %shard_map.91 = bf16[384,2048]{1,0:T(8,128)(2,1)S(1)} custom-call(bf16[1,768,1024]{2,1,0:T(8,128)(2,1)} %tok_hbm.1, f32[1,2048]{1,0:T(1,128)} %bitcast.21, bf16[512,2048]{1,0:T(8,128)(2,1)} %bitcast.15, bf16[128,2048]{1,0:T(8,128)(2,1)} %bitcast.19, bf16[128,2048]{1,0:T(8,128)(2,1)} %bitcast.20, f32[8]{0:T(128)} %sink_hbm.1, bf16[8192,128]{1,0:T(8,128)(2,1)} %bitcast.16, ...), custom_call_target="tpu_custom_call" | custom-call | tf_op jit(solution)/shard_map/pallas_call | solution.py:452
  36.0 1.1 %copy.11 = bf16[1,384,2048]{2,1,0:T(8,128)(2,1)} copy(bf16[1,384,2048]{2,1,0:T(8,128)(2,1)S(1)} %bitcast.14) | data formatting | bytes 3145728

commit v4 on v3

--- a/solution.py
+++ b/solution.py
@@ -12,6 +12,7 @@
 TAIL = 16
 GROUP = 4
 CHUNKS = 3
+PARTS = ((4, 1), (5, 1), (2, 2), (0, 2))
 OUT_CHUNKS = 2
 NEG = -1e30
 BF16 = jnp.bfloat16
@@ -24,7 +25,7 @@
     tok_hbm, gain_hbm, wq_hbm, wk_hbm, wv_hbm, sink_hbm, wp_hbm, wa_hbm, wpo_hbm,
     outbuf,
     tok, nrm0, nrm1, nrm2, gain_ref, sink_ref, wqkv, wpraw, wp, wo, qt, kx, vt, px, att, l3, bt,
-    sbuf, pbuf,
+    sbuf, pbuf, masks,
     kin, vin, pin, ktail, vtail, ptail, totout, totin, carryout, carryin,
     own0, own1, sendbuf, recvbuf,
     tok_sem, w_sem, tsend, trecv, tail_send, tail_recv, tot_send, tot_recv,
@@ -46,10 +47,12 @@
     gi = lax.rem(z, GROUP)
     base = z - gi
 
+    mine = pl.ds(pl.multiple_of(me * half, half), half)
+
     def tok_copy(c):
         return pltpu.make_async_copy(
             tok_hbm.at[0, pl.ds(c * crow, crow), :],
-            tok.at[pl.ds(c * crow, crow), pl.ds(pl.multiple_of(me * half, half), half)],
+            tok.at[pl.ds(c * crow, crow), mine],
             tok_sem.at[c],
         )
 
@@ -66,10 +69,15 @@
     ]
     barrier = pltpu.get_barrier_semaphore()
     pl.semaphore_signal(barrier, inc=1, device_id={"tp": other}, device_id_type=MESH)
-    for c in reversed(range(CHUNKS)):
-        tok_copy(c).start()
-    for load in (*loads[6:], *loads[1:4], loads[0], *loads[4:6]):
+    tok_copy(2).start()
+    for load in (*loads[6:], *loads[1:4]):
         load.start()
+
+    @pl.when(me == 1)
+    def _():
+        tok_copy(1).start()
+        tok_copy(0).start()
+
 
     def sends_to(d):
         inside = gi + d < GROUP
@@ -88,18 +96,30 @@
     behind = gi + jnp.where(base > 0, 1, 0)
     pl.semaphore_wait(barrier, 1 + behind)
 
-    def tok_send(c):
+    def tok_send(n, loaded=False):
+        first, count = PARTS[n]
+        spot = pl.ds(first * WINDOW, count * WINDOW)
         return pltpu.make_async_remote_copy(
-            src_ref=tok_hbm.at[0, pl.ds(c * crow, crow), :],
-            dst_ref=tok.at[pl.ds(c * crow, crow), pl.ds(pl.multiple_of(me * half, half), half)],
-            send_sem=tsend.at[c],
-            recv_sem=trecv.at[c],
+            src_ref=tok.at[spot, mine] if loaded else tok_hbm.at[0, spot, :],
+            dst_ref=tok.at[spot, mine],
+            send_sem=tsend.at[n],
+            recv_sem=trecv.at[n],
             device_id={"tp": other},
             device_id_type=MESH,
         )
 
-    for c in reversed(range(CHUNKS)):
-        tok_send(c).start()
+    @pl.when(me == 0)
+    def _():
+        for n in range(len(PARTS)):
+            tok_send(n).start()
+
+    @pl.when(me == 1)
+    def _():
+        for c in reversed(range(CHUNKS)):
+            tok_copy(c).wait()
+        for n in range(len(PARTS)):
+            tok_send(n, True).start()
+
     for d in range(1, GROUP + 1):
 
         @pl.when(hears_from(d))
@@ -123,21 +143,24 @@
                     64 * g : 64 * g + 64, 128 * s : 128 * s + 128
                 ]
 
-    def norm(c):
-        for n in range(crow // 16):
+    def norm(c, low=0, high=crow // 16):
+        for n in range(low, high):
             x = tok[c * crow + 16 * n : c * crow + 16 * (n + 1), :].astype(F32)
             mean = jnp.sum(x * x, axis=1, keepdims=True) * (1.0 / width)
             scale = lax.rsqrt(mean + 1e-06)
             nrm[c][16 * n : 16 * (n + 1), :] = (x * scale * gain).astype(BF16)
 
-    def pool_in(c):
+    def pool_in(c, part=None):
         lo = c * crow
-        pooled_in = jnp.dot(nrm[c][...], wp[...], preferred_element_type=F32).astype(BF16)
-        px[WINDOW + lo : WINDOW + lo + crow, :] = pooled_in
-        for b in range(crow // WINDOW):
-            piece = pooled_in[b * WINDOW : (b + 1) * WINDOW, 384:].astype(F32)
-            n = c * (crow // WINDOW) + b
-            bt[n : n + 1, :] = jnp.sum(piece, axis=0, keepdims=True)
+        for p in (0, 1) if part is None else (part,):
+            cols = slice(256 * p, 256 * (p + 1))
+            pooled_in = jnp.dot(nrm[c][...], wp[:, cols], preferred_element_type=F32).astype(BF16)
+            px[WINDOW + lo : WINDOW + lo + crow, cols] = pooled_in
+            if p == 1:
+                for b in range(crow // WINDOW):
+                    piece = pooled_in[b * WINDOW : (b + 1) * WINDOW, 128:].astype(F32)
+                    n = c * (crow // WINDOW) + b
+                    bt[n : n + 1, :] = jnp.sum(piece, axis=0, keepdims=True)
 
     def qkv_of(c):
         lo = c * crow
@@ -198,7 +221,8 @@
         return (lax.broadcasted_iota(jnp.int32, (WINDOW, 1), 0) + first).astype(F32)
 
     here = keyi <= posi
-    quarter = here[:, :WINDOW]
+    masks[1] = jnp.where(here, 1.0, 0.0).astype(BF16)
+    masks[0] = jnp.where(here, 0.0, 1.0).astype(BF16)
 
     def scores(n, b, h):
         lo = b * WINDOW
@@ -218,19 +242,20 @@
         sbuf[n] = jnp.where(here, s[WINDOW:], before)
 
     def weights(n, b, h):
-        for j in range(group):
-            s = sbuf[n, :, j * WINDOW : (j + 1) * WINDOW]
-            sink = jnp.full((1, WINDOW), sink_ref[group * h + j], F32)
+        for j in range(0, group, 2):
+            s = sbuf[n, :, j * WINDOW : (j + 2) * WINDOW]
+            sink = jnp.concatenate(
+                [jnp.full((1, WINDOW), sink_ref[group * h + j + i], F32) for i in range(2)], axis=1
+            )
             top = jnp.maximum(jnp.max(s, axis=0, keepdims=True), sink)
             e = jnp.exp(s - top)
             tot = jnp.sum(e, axis=0, keepdims=True) + jnp.exp(sink - top)
-            pbuf[n, :, j * WINDOW : (j + 1) * WINDOW] = (e * (1.0 / tot)).astype(BF16)
+            pbuf[n, :, j * WINDOW : (j + 2) * WINDOW] = (e * (1.0 / tot)).astype(BF16)
 
     def attend(n, b, h):
         lo = b * WINDOW
         w = pbuf[n]
-        blank = jnp.zeros_like(w)
-        wt = jnp.concatenate([jnp.where(here, blank, w), jnp.where(here, w, blank)], axis=0)
+        wt = jnp.concatenate([w * masks[0], w * masks[1]], axis=0)
         o = jnp.dot(
             vt[64 * h : 64 * (h + 1), lo : lo + 2 * WINDOW], wt, preferred_element_type=F32
         )
@@ -238,56 +263,81 @@
         att[lo : lo + WINDOW, 64 * group * h : 64 * group * (h + 1)] = jnp.transpose(o).astype(BF16)
 
     def pool(b):
-        lo = b * WINDOW
-        count = counts(b)
+        spots = [n * WINDOW for n in (b, b + 1)]
+
+        def both(g):
+            return jnp.concatenate(
+                [px[lo : lo + 2 * WINDOW, 128 * g : 128 * (g + 1)] for lo in spots], axis=1
+            )
+
+        means = []
         for g in range(3):
-            near = px[lo : lo + 2 * WINDOW, 128 * g : 128 * (g + 1)]
+            near = both(g)
             sums = jnp.dot(bands[g], near, preferred_element_type=F32)
-            mean = sums * (1.0 / jnp.minimum(count, float(REACHES[g])))
-            att[lo : lo + WINDOW, qn + 128 * g : qn + 128 * (g + 1)] = (
-                mean - near[WINDOW:].astype(F32)
-            ).astype(BF16)
-        near = px[lo : lo + 2 * WINDOW, 384:512]
-        l3[lo : lo + WINDOW, :] = jnp.dot(bands[3], near, preferred_element_type=F32)
-
-    def blocks(which, beside=()):
+            here_in = near[WINDOW:].astype(F32)
+            for n in range(2):
+                part = slice(n * WINDOW, (n + 1) * WINDOW)
+                scale = 1.0 / jnp.minimum(counts(b + n), float(REACHES[g]))
+                means.append((sums[:, part] * scale - here_in[:, part]).astype(BF16))
+        for n, lo in enumerate(spots):
+            att[lo : lo + WINDOW, qn : qn + 256] = jnp.concatenate([means[n], means[2 + n]], axis=1)
+            att[lo : lo + WINDOW, qn + 256 : qn + 384] = means[4 + n]
+        sums = jnp.dot(bands[3], both(3), preferred_element_type=F32)
+        for n, lo in enumerate(spots):
+            l3[lo : lo + WINDOW, :] = sums[:, n * WINDOW : (n + 1) * WINDOW]
+
+    def blocks(which, spots, beside):
         chains = [(b, h) for b in which for h in range(kv)]
         last = len(chains)
         beside = list(beside)
-        for n in range(last + 2):
+        for n in range(last + 6):
             if n < last:
                 scores(n, *chains[n])
-            if 0 <= n - 1 < last:
-                weights(n - 1, *chains[n - 1])
-            if n % 2 == 1 and beside:
-                step, chunk = beside.pop(0)
-                step(chunk)
-            if 0 <= n - 2 < last:
-                attend(n - 2, *chains[n - 2])
-                if chains[n - 2][1] == 0:
-                    pool(chains[n - 2][0])
+            if 0 <= n - 3 < last:
+                weights(n - 3, *chains[n - 3])
+            while spots and spots[0] == n:
+                spots = spots[1:]
+                step, *what = beside.pop(0)
+                step(*what)
+            if 0 <= n - 6 < last:
+                attend(n - 6, *chains[n - 6])
 
     loads[6].wait()
     gain = gain_ref[...]
-    tok_copy(2).wait()
-    tok_send(2).wait_recv()
-    norm(2)
-    tok_copy(1).wait()
+
+    @pl.when(me == 0)
+    def _():
+        tok_copy(2).wait()
+        tok_copy(1).start()
+        tok_copy(0).start()
+
+    loads[0].start()
+    tok_send(0).wait_recv()
+    norm(2, 0, crow // 32)
     tok_send(1).wait_recv()
+    norm(2, crow // 32)
     for load in loads[1:4]:
         load.wait()
 
-    norm(1)
     qkv_of(2)
 
-    tok_copy(0).wait()
-    tok_send(0).wait_recv()
+    loads[4].start()
+    loads[5].start()
+
+    @pl.when(me == 0)
+    def _():
+        tok_copy(1).wait()
+        tok_copy(0).wait()
+
+    tok_send(2).wait_recv()
+    tok_send(3).wait_recv()
     loads[0].wait()
-    norm(0)
     for r in range(width // 128):
         sort_one(r)
+    norm(1)
+    pool_in(2)
+    norm(0)
     qkv_of(1)
-    pool_in(2)
 
     ktail[...] = kx[rows : rows + WINDOW, :]
     vtail[...] = vt[:, rows : rows + WINDOW]
@@ -304,7 +354,7 @@
 
     loads[7].wait()
 
-    blocks(range(nb - 1, nb // 2 - 1, -1), ((pool_in, 1), (qkv_of, 0), (pool_in, 0)))
+    blocks(range(nb - 1, nb // 2 - 1, -1), (1, 3, 5), ((pool_in, 1, 1), (qkv_of, 0), (pool_in, 0, 1)))
 
     total = jnp.sum(bt[0:nb, :], axis=0, keepdims=True)
     totout[...] = jnp.broadcast_to(total, totout.shape)
@@ -324,7 +374,7 @@
         vt[:, 0:WINDOW] = vin[...]
         px[WINDOW - TAIL : WINDOW, 0:384] = pin[...]
 
-    blocks(range(nb // 2 - 1, -1, -1))
+    blocks(range(nb // 2 - 1, -1, -1), (5, 5, 9, 10, 11), ((pool_in, 1, 0), (pool_in, 0, 0), (pool, 4), (pool, 2), (pool, 0)))
 
     for d in range(1, GROUP):
 
@@ -400,8 +450,8 @@
         out_copy(n).wait_recv()
         add(n)
 
-    for c in range(CHUNKS):
-        tok_send(c).wait_send()
+    for n in range(len(PARTS)):
+        tok_send(n).wait_send()
     for d in range(1, GROUP):
 
         @pl.when(gi + d < GROUP)
@@ -474,6 +524,7 @@
             vm((8, 128), F32),
             vm((6, WINDOW, 512), F32),
             vm((6, WINDOW, 512), BF16),
+            vm((2, WINDOW, 512), BF16),
             vm((WINDOW, kn), BF16),
             vm((kn, WINDOW), BF16),
             vm((TAIL, 384), BF16),
@@ -490,8 +541,8 @@
             vm((orow, width), BF16),
             dma((CHUNKS,)),
             dma((8,)),
-            dma((CHUNKS,)),
-            dma((CHUNKS,)),
+            dma((len(PARTS),)),
+            dma((len(PARTS),)),
             dma((3,)),
             dma((3,)),
             dma((GROUP - 1,)),

time: 37.3 us -> 36.4 us (0.976)
  Pallas kernels: 36 us -> 35.2 us
    pallas_call x1, Pallas kernels: 36 us -> 35.2 us  [shards(): pl.pallas_call(kernel, out_shape=pltpu.VMEM((orow, width), BF16), in_spec...]
where the time goes in v4:
time: 36.4 us; the launch traced here: 36.3 us
  Pallas kernels  35.2 us (97%)
  local copies, waits for them, and re-layouts  1.15 us (3%)
    pallas_call x1, Pallas kernels, shards(): pl.pallas_call(kernel, out_shape=pltpu.VMEM((orow, width), BF16), in_spec...  35.2 us
    unnamed x1, local copies, waits for them, and re-layouts  1.15 us

profile of v4, /device:TPU:33, one launch (start us, length us, event | category | flops | bytes accessed | tf_op | source)
XLA Modules:
  0.0 36.3 jit_solution(1913913752641107135)
XLA Ops:
  0.0 35.2 %shard_map.91 = bf16[384,2048]{1,0:T(8,128)(2,1)S(1)} custom-call(bf16[1,768,1024]{2,1,0:T(8,128)(2,1)} %tok_hbm.1, f32[1,2048]{1,0:T(1,128)} %bitcast.21, bf16[512,2048]{1,0:T(8,128)(2,1)} %bitcast.15, bf16[128,2048]{1,0:T(8,128)(2,1)} %bitcast.19, bf16[128,2048]{1,0:T(8,128)(2,1)} %bitcast.20, f32[8]{0:T(128)} %sink_hbm.1, bf16[8192,128]{1,0:T(8,128)(2,1)} %bitcast.16, ...), custom_call_target="tpu_custom_call" | custom-call | tf_op jit(solution)/shard_map/pallas_call | solution.py:502
  35.2 1.1 %copy.11 = bf16[1,384,2048]{2,1,0:T(8,128)(2,1)} copy(bf16[1,384,2048]{2,1,0:T(8,128)(2,1)S(1)} %bitcast.14) | data formatting | bytes 3145728

commit v5 on v4

--- a/solution.py
+++ b/solution.py
@@ -70,7 +70,7 @@
     barrier = pltpu.get_barrier_semaphore()
     pl.semaphore_signal(barrier, inc=1, device_id={"tp": other}, device_id_type=MESH)
     tok_copy(2).start()
-    for load in (*loads[6:], *loads[1:4]):
+    for load in (*loads[6:], loads[0]):
         load.start()
 
     @pl.when(me == 1)
@@ -308,34 +308,37 @@
     @pl.when(me == 0)
     def _():
         tok_copy(2).wait()
+
+    loads[0].wait()
+
+    @pl.when(me == 0)
+    def _():
         tok_copy(1).start()
         tok_copy(0).start()
 
-    loads[0].start()
-    tok_send(0).wait_recv()
-    norm(2, 0, crow // 32)
-    tok_send(1).wait_recv()
-    norm(2, crow // 32)
+    for load in loads[1:4]:
+        load.start()
+    for n in range(2):
+        tok_send(n).wait_recv()
+        norm(2, n * crow // 32, (n + 1) * crow // 32)
+        for r in range(n * width // 256, (n + 1) * width // 256):
+            sort_one(r)
+
+    loads[4].start()
+    loads[5].start()
+    pool_in(2)
+
+    @pl.when(me == 0)
+    def _():
+        tok_copy(1).wait()
+        tok_copy(0).wait()
+
+    tok_send(2).wait_recv()
+    tok_send(3).wait_recv()
     for load in loads[1:4]:
         load.wait()
-
+    norm(1)
     qkv_of(2)
-
-    loads[4].start()
-    loads[5].start()
-
-    @pl.when(me == 0)
-    def _():
-        tok_copy(1).wait()
-        tok_copy(0).wait()
-
-    tok_send(2).wait_recv()
-    tok_send(3).wait_recv()
-    loads[0].wait()
-    for r in range(width // 128):
-        sort_one(r)
-    norm(1)
-    pool_in(2)
     norm(0)
     qkv_of(1)
 

time: 36.4 us -> 36.7 us (level)
  no operation moved by 1% of the time
where the time goes in v5:
time: 36.7 us; the launch traced here: 36.5 us
  Pallas kernels  35.4 us (96%)
  local copies, waits for them, and re-layouts  1.15 us (3%)
    pallas_call x1, Pallas kernels, shards(): pl.pallas_call(kernel, out_shape=pltpu.VMEM((orow, width), BF16), in_spec...  35.4 us
    unnamed x1, local copies, waits for them, and re-layouts  1.15 us

profile of v5, /device:TPU:33, one launch (start us, length us, event | category | flops | bytes accessed | tf_op | source)
XLA Modules:
  0.0 36.5 jit_solution(16067054239252510619)
XLA Ops:
  0.0 35.4 %shard_map.91 = bf16[384,2048]{1,0:T(8,128)(2,1)S(1)} custom-call(bf16[1,768,1024]{2,1,0:T(8,128)(2,1)} %tok_hbm.1, f32[1,2048]{1,0:T(1,128)} %bitcast.21, bf16[512,2048]{1,0:T(8,128)(2,1)} %bitcast.15, bf16[128,2048]{1,0:T(8,128)(2,1)} %bitcast.19, bf16[128,2048]{1,0:T(8,128)(2,1)} %bitcast.20, f32[8]{0:T(128)} %sink_hbm.1, bf16[8192,128]{1,0:T(8,128)(2,1)} %bitcast.16, ...), custom_call_target="tpu_custom_call" | custom-call | tf_op jit(solution)/shard_map/pallas_call | solution.py:505
  35.4 1.1 %copy.11 = bf16[1,384,2048]{2,1,0:T(8,128)(2,1)} copy(bf16[1,384,2048]{2,1,0:T(8,128)(2,1)S(1)} %bitcast.14) | data formatting | bytes 3145728

commit v6 on v5

--- a/solution.py
+++ b/solution.py
@@ -57,15 +57,35 @@
         )
 
     qn, kn = wq_hbm.shape[0], wk_hbm.shape[0]
+    class Split:
+        def __init__(self, src, dst, low, pieces, first):
+            step = src.shape[0] // pieces
+            self.copies = [
+                pltpu.make_async_copy(
+                    src.at[pl.ds(n * step, step)],
+                    dst.at[pl.ds(low + n * step, step)],
+                    w_sem.at[first + n],
+                )
+                for n in range(pieces)
+            ]
+
+        def start(self):
+            for copy in self.copies:
+                copy.start()
+
+        def wait(self):
+            for copy in self.copies:
+                copy.wait()
+
     loads = [
-        pltpu.make_async_copy(wp_hbm, wpraw, w_sem.at[0]),
-        pltpu.make_async_copy(wq_hbm, wqkv.at[pl.ds(0, qn)], w_sem.at[1]),
-        pltpu.make_async_copy(wk_hbm, wqkv.at[pl.ds(qn, kn)], w_sem.at[2]),
-        pltpu.make_async_copy(wv_hbm, wqkv.at[pl.ds(qn + kn, kn)], w_sem.at[3]),
-        pltpu.make_async_copy(wa_hbm, wo.at[pl.ds(0, qn)], w_sem.at[4]),
-        pltpu.make_async_copy(wpo_hbm, wo.at[pl.ds(qn, wo.shape[0] - qn)], w_sem.at[5]),
-        pltpu.make_async_copy(gain_hbm, gain_ref, w_sem.at[6]),
-        pltpu.make_async_copy(sink_hbm, sink_ref, w_sem.at[7]),
+        Split(wp_hbm, wpraw, 0, 8, 0),
+        Split(wq_hbm, wqkv, 0, 4, 8),
+        Split(wk_hbm, wqkv, qn, 1, 12),
+        Split(wv_hbm, wqkv, qn + kn, 1, 13),
+        Split(wa_hbm, wo, 0, 1, 14),
+        Split(wpo_hbm, wo, qn, 1, 15),
+        pltpu.make_async_copy(gain_hbm, gain_ref, w_sem.at[16]),
+        pltpu.make_async_copy(sink_hbm, sink_ref, w_sem.at[17]),
     ]
     barrier = pltpu.get_barrier_semaphore()
     pl.semaphore_signal(barrier, inc=1, device_id={"tp": other}, device_id_type=MESH)
@@ -304,20 +324,16 @@
 
     loads[6].wait()
     gain = gain_ref[...]
+    for load in loads[1:4]:
+        load.start()
 
     @pl.when(me == 0)
     def _():
         tok_copy(2).wait()
-
-    loads[0].wait()
-
-    @pl.when(me == 0)
-    def _():
         tok_copy(1).start()
         tok_copy(0).start()
 
-    for load in loads[1:4]:
-        load.start()
+    loads[0].wait()
     for n in range(2):
         tok_send(n).wait_recv()
         norm(2, n * crow // 32, (n + 1) * crow // 32)
@@ -543,7 +559,7 @@
             vm((orow, width), BF16),
             vm((orow, width), BF16),
             dma((CHUNKS,)),
-            dma((8,)),
+            dma((18,)),
             dma((len(PARTS),)),
             dma((len(PARTS),)),
             dma((3,)),

time: 36.7 us -> 36.3 us (0.989)
  Pallas kernels: 35.4 us -> 35 us
    pallas_call x1, Pallas kernels: 35.4 us -> 35 us  [shards(): pl.pallas_call(kernel, out_shape=pltpu.VMEM((orow, width), BF16), in_spec...]
where the time goes in v6:
time: 36.3 us; the launch traced here: 36.1 us
  Pallas kernels  35 us (96%)
  local copies, waits for them, and re-layouts  1.15 us (3%)
    pallas_call x1, Pallas kernels, shards(): pl.pallas_call(kernel, out_shape=pltpu.VMEM((orow, width), BF16), in_spec...  35 us
    unnamed x1, local copies, waits for them, and re-layouts  1.15 us

profile of v6, /device:TPU:33, one launch (start us, length us, event | category | flops | bytes accessed | tf_op | source)
XLA Modules:
  0.0 36.1 jit_solution(11979704711709097295)
XLA Ops:
  0.0 35.0 %shard_map.91 = bf16[384,2048]{1,0:T(8,128)(2,1)S(1)} custom-call(bf16[1,768,1024]{2,1,0:T(8,128)(2,1)} %tok_hbm.1, f32[1,2048]{1,0:T(1,128)} %bitcast.21, bf16[512,2048]{1,0:T(8,128)(2,1)} %bitcast.15, bf16[128,2048]{1,0:T(8,128)(2,1)} %bitcast.19, bf16[128,2048]{1,0:T(8,128)(2,1)} %bitcast.20, f32[8]{0:T(128)} %sink_hbm.1, bf16[8192,128]{1,0:T(8,128)(2,1)} %bitcast.16, ...), custom_call_target="tpu_custom_call" | custom-call | tf_op jit(solution)/shard_map/pallas_call | solution.py:521
  35.0 1.1 %copy.11 = bf16[1,384,2048]{2,1,0:T(8,128)(2,1)} copy(bf16[1,384,2048]{2,1,0:T(8,128)(2,1)S(1)} %bitcast.14) | data formatting | bytes 3145728

commit v7 on v6

--- a/solution.py
+++ b/solution.py
@@ -324,12 +324,16 @@
 
     loads[6].wait()
     gain = gain_ref[...]
+
+    @pl.when(me == 0)
+    def _():
+        tok_copy(2).wait()
+
     for load in loads[1:4]:
         load.start()
 
     @pl.when(me == 0)
     def _():
-        tok_copy(2).wait()
         tok_copy(1).start()
         tok_copy(0).start()
 

time: 36.3 us -> 36.5 us (level)
  no operation moved by 1% of the time
where the time goes in v7:
time: 36.5 us; the launch traced here: 36.3 us
  Pallas kernels  35.2 us (96%)
  local copies, waits for them, and re-layouts  1.15 us (3%)
    pallas_call x1, Pallas kernels, shards(): pl.pallas_call(kernel, out_shape=pltpu.VMEM((orow, width), BF16), in_spec...  35.2 us
    unnamed x1, local copies, waits for them, and re-layouts  1.15 us

profile of v7, /device:TPU:33, one launch (start us, length us, event | category | flops | bytes accessed | tf_op | source)
XLA Modules:
  0.0 36.3 jit_solution(13332706141762797962)
XLA Ops:
  0.0 35.2 %shard_map.91 = bf16[384,2048]{1,0:T(8,128)(2,1)S(1)} custom-call(bf16[1,768,1024]{2,1,0:T(8,128)(2,1)} %tok_hbm.1, f32[1,2048]{1,0:T(1,128)} %bitcast.21, bf16[512,2048]{1,0:T(8,128)(2,1)} %bitcast.15, bf16[128,2048]{1,0:T(8,128)(2,1)} %bitcast.19, bf16[128,2048]{1,0:T(8,128)(2,1)} %bitcast.20, f32[8]{0:T(128)} %sink_hbm.1, bf16[8192,128]{1,0:T(8,128)(2,1)} %bitcast.16, ...), custom_call_target="tpu_custom_call" | custom-call | tf_op jit(solution)/shard_map/pallas_call | solution.py:525
  35.2 1.1 %copy.11 = bf16[1,384,2048]{2,1,0:T(8,128)(2,1)} copy(bf16[1,384,2048]{2,1,0:T(8,128)(2,1)S(1)} %bitcast.14) | data formatting | bytes 3145728
